TPU v7x, 256 devices: a whole 4x4x8 slice. The times are simulated.
256 devices in a mesh: sp: 16 (over y, x), tp: 16 (over z, core).
Axes of the slice: x: 4, y: 4, z: 8, core: 2. Of those that a mesh axis runs over, the one named last changes fastest.
Arguments:
- queries: bfloat16 [12288, 16, 128], P('sp', 'tp'), may hold values from -240 to 240
- key_pairs: bfloat16 [12288, 16, 128], P('sp', 'tp'), may hold values from -11 to 11
- head_values: bfloat16 [12288, 16, 128], P('sp', 'tp'), may hold values from -6 to 6
- lambdas: float32 [16], P('tp'), may hold values from 0.3 to 0.8
- head_gain: float32 [128], replicated, may hold values from 0.1 to 1.9
- out_weight: bfloat16 [2048, 2048], replicated, may hold values from -0.125 to 0.125
- residual: bfloat16 [12288, 2048], P(('sp', 'tp')), may hold values from -6 to 6
- norm_gain: float32 [2048], replicated, may hold values from 0.1 to 1.9
- expert_ids: int32 [12288, 2], P(('sp', 'tp')), may hold values from 0 to 31, all different within a row; in each aligned block of 48 rows (0 to 47, 48 to 95, ...) at most 4 rows name the same one
- route_weights: float32 [12288, 2], P(('sp', 'tp')), may hold values from 0.2 to 1
- gate_weight: bfloat16 [32, 2048, 2048], P('sp', None, 'tp'), may hold values from -0.125 to 0.125
- up_weight: bfloat16 [32, 2048, 2048], P('sp', None, 'tp'), may hold values from -0.125 to 0.125
- down_weight: bfloat16 [32, 2048, 2048], P('sp', 'tp'), may hold values from -0.125 to 0.125
Outputs:
- merged: bfloat16 [12288, 2048], P(('sp', 'tp'))
Inputs may be any that keep to these rules, and one draw needn't show every extreme that they name: `expert_ids`: within the rows of one device each expert is named at most 4 times, and exactly 4 times in some device.
All inputs are finite; a program needn't handle non-finite values.
Results may differ from a plain program's by a relative error of at most 0.019.
Values may be sent and summed in bfloat16 or wider, within the bound.
A program may use at most 128 MiB of HBM per device.

v0:
```python
import math

import jax
import jax.numpy as jnp
from jax import lax
from jax.sharding import Mesh
from jax.sharding import PartitionSpec as P

TP = ("tp_0", "tp_1")
SP_TP = ("sp", "tp_0", "tp_1")


def side_by_side(arrays, axis, dim, along):
    widths = [a.shape[along] for a in arrays]
    both = jnp.concatenate(arrays, axis=along)
    whole = lax.all_gather(both, axis, axis=dim, tiled=True)
    return tuple(jnp.split(whole, [sum(widths[:k]) for k in range(1, len(widths))], axis=along))


def sum_in_order(parts, axes, turns):
    shape = [lax.axis_size(a) for a in axes]
    parts = parts.reshape(*shape, *parts.shape[1:])
    parts = parts.transpose(*turns, *range(len(axes), parts.ndim))
    parts = parts.reshape(-1, *parts.shape[len(axes) :])
    for k in turns:
        parts = lax.psum_scatter(parts, axes[k], scatter_dimension=0, tiled=True)
    return parts[0]


def in_blocks(value, dim, length):
    before, after = (value.shape[:dim], value.shape[dim + 1 :])
    return jnp.moveaxis(value.reshape(*before, length, -1, *after), dim, 0)


def scatter_axes(value, axes, turns, dim):
    length = lax.axis_size(axes)
    return sum_in_order(in_blocks(value, dim, length), axes, turns)


def shards(
    queries,
    key_pairs,
    head_values,
    lambdas,
    head_gain,
    out_weight,
    residual,
    norm_gain,
    expert_ids,
    route_weights,
    gate_weight,
    up_weight,
    down_weight,
):
    tokens_here, heads_here, pair_width = queries.shape
    half_width = pair_width // 2
    value_width = head_values.shape[2]
    score_scale = half_width ** (-0.5)
    query_pos = lax.axis_index("sp") * tokens_here + jnp.arange(tokens_here, dtype=jnp.int32)
    split_queries = queries.reshape(tokens_here, heads_here, 2, half_width)
    start_state = (
        jnp.full((2, heads_here, tokens_here), -1e30, jnp.float32),
        jnp.zeros((2, heads_here, tokens_here), jnp.float32),
        jnp.zeros((2, heads_here, tokens_here, value_width), jnp.float32),
    )
    key_piece, value_piece = side_by_side((key_pairs, head_values), "sp", 0, 1)
    span_rows = key_piece.shape[0]
    width_rows = math.gcd(span_rows, 512)

    def block_step(block_index, state):
        running_max, totals, summed = state
        offset = block_index * width_rows
        key_block = lax.dynamic_slice_in_dim(key_piece, offset, width_rows, 0).reshape(
            width_rows, heads_here, 2, half_width
        )
        value_block = lax.dynamic_slice_in_dim(value_piece, offset, width_rows, 0)
        key_pos = offset + jnp.arange(width_rows, dtype=jnp.int32)
        allowed = key_pos[None, :] <= query_pos[:, None]
        scores = (
            jnp.einsum(
                "qhcd,khcd->chqk", split_queries, key_block, preferred_element_type=jnp.float32
            )
            * score_scale
        )
        scores = jnp.where(allowed[None, None], scores, -jnp.inf)
        fresh_max = jnp.maximum(running_max, jnp.max(scores, axis=3))
        decay = jnp.exp(running_max - fresh_max)
        weights = jnp.exp(scores - fresh_max[..., None])
        totals = totals * decay + jnp.sum(weights, axis=3)
        summed = summed * decay[..., None] + jnp.einsum(
            "chqk,khv->chqv",
            weights.astype(jnp.bfloat16),
            value_block,
            preferred_element_type=jnp.float32,
        )
        return (fresh_max, totals, summed)

    def through(state):
        return lax.fori_loop(0, span_rows // width_rows, block_step, state)

    def untouched(state):
        return state

    running_max, totals, summed = lax.cond(
        jnp.int32(0) <= query_pos[-1], through, untouched, start_state
    )
    mixed = (
        summed[0] / totals[0][..., None] - lambdas[:, None, None] * summed[1] / totals[1][..., None]
    )
    normed_heads = (
        mixed * lax.rsqrt(jnp.mean(mixed * mixed, axis=2, keepdims=True) + 1e-06) * head_gain
    )
    attended = (
        jnp.transpose(normed_heads, (1, 0, 2))
        .reshape(tokens_here, heads_here * value_width)
        .astype(jnp.bfloat16)
    )
    rows_here = residual.shape[0]
    regrouped = lax.all_to_all(attended, TP, split_axis=0, concat_axis=1, tiled=True)
    projected = jnp.dot(regrouped, out_weight, preferred_element_type=jnp.float32)
    updated = (residual.astype(jnp.float32) + projected).astype(jnp.bfloat16)
    widened = updated.astype(jnp.float32)
    normed = (
        widened * lax.rsqrt(jnp.mean(widened * widened, axis=1, keepdims=True) + 1e-06) * norm_gain
    ).astype(jnp.bfloat16)
    route_count = expert_ids.shape[1]
    local_experts = gate_weight.shape[0]
    sp_count = lax.axis_size("sp")
    expert_count = local_experts * sp_count
    capacity = max(2, 4 * rows_here * route_count // (3 * expert_count))
    model_width = normed.shape[1]
    flat_ids = expert_ids.reshape(-1)
    indicator = (flat_ids[:, None] == jnp.arange(expert_count, dtype=jnp.int32)[None, :]).astype(
        jnp.int32
    )
    ranking = jnp.sum(jnp.cumsum(indicator, axis=0) * indicator, axis=1) - 1
    slots = flat_ids * capacity + ranking
    sources = jnp.arange(rows_here * route_count, dtype=jnp.int32) // route_count
    outgoing = (
        jnp.zeros((expert_count * capacity, model_width), jnp.bfloat16)
        .at[slots]
        .set(normed[sources])
    )
    arrived = lax.all_to_all(
        outgoing.reshape(sp_count, local_experts, capacity, model_width),
        "sp",
        split_axis=0,
        concat_axis=0,
        tiled=True,
    )
    piece_rows = lax.all_gather(arrived[None], TP, axis=0, tiled=True)
    gate_part = jnp.einsum(
        "tsecd,edf->tsecf", piece_rows, gate_weight, preferred_element_type=jnp.float32
    )
    up_part = jnp.einsum(
        "tsecd,edf->tsecf", piece_rows, up_weight, preferred_element_type=jnp.float32
    )
    inner_rows = (jax.nn.silu(gate_part) * up_part).astype(jnp.bfloat16)
    partial_value = jnp.einsum(
        "tsecf,efd->tsecd", inner_rows, down_weight, preferred_element_type=jnp.float32
    )
    reduced = (
        scatter_axes(partial_value.astype(jnp.bfloat16), TP, (1, 0), 0)
        .astype(jnp.float32)
        .astype(jnp.bfloat16)
    )
    returned = lax.all_to_all(reduced[0], "sp", split_axis=0, concat_axis=0, tiled=True)
    picked = (
        returned.reshape(expert_count * capacity, model_width)[slots]
        .astype(jnp.float32)
        .reshape(rows_here, route_count, model_width)
    )
    moe_sum = jnp.sum(picked * route_weights[:, :, None], axis=1)
    return (updated.astype(jnp.float32) + moe_sum).astype(jnp.bfloat16)


def solution(mesh):
    torus = Mesh(mesh.devices.reshape(mesh.shape["sp"], 8, 2), ("sp", "tp_0", "tp_1"))
    in_specs = (
        P("sp", TP, None),
        P("sp", TP, None),
        P("sp", TP, None),
        P(TP),
        P(),
        P(),
        P(SP_TP, None),
        P(),
        P(SP_TP, None),
        P(SP_TP, None),
        P("sp", None, TP),
        P("sp", None, TP),
        P("sp", TP, None),
    )
    out_specs = P(SP_TP, None)
    return jax.shard_map(
        shards, mesh=torus, in_specs=in_specs, out_specs=out_specs, check_vma=False
    )
```

profile of v0, /device:TPU:2, one launch (start us, length us, event | category | flops | bytes accessed | tf_op | source)
XLA Modules:
  0.0 544.5 jit_solution(14466125331145611714)
XLA Ops:
  13.2 65.7 %all-gather.4.cloned.1.call-done = bf16[12288,2,128]{0,2,1:T(8,128)(2,1)} async-done(((bf16[768,2,128]{0,2,1:T(8,128)(2,1)}), bf16[12288,2,128]{0,2,1:T(8,128)(2,1)}) %all-gather.4.cloned.1.call-update) | async-done | bytes 6291472 | tf_op jit(solution)/shard_map/all_gather | solution.py:16
  78.9 222.9 %conditional.1 = (f32[2,1,768]{2,0,1:T(2,128)}, f32[1,1,768,128]{3,2,1,0:T(8,128)S(1)}, f32[1,1,768,128]{3,2,1,0:T(8,128)S(1)}) conditional(s32[]{:T(128)} %bitcast.1, () %tuple.27, (bf16[12288,2,128]{0,2,1:T(8,128)(2,1)}, bf16[768,1,128]{2,0,1:T(8,128)(2,1)}, s32[768]{0:T(1024)S(1)}) %tuple.28), branch_computations={%region_0.0_spmd.clone, %region_1.6_spmd.clone} | conditional | flops 311633408 | bytes 42900848 | solution.py:104
  78.9 6.2 %fusion.65 = (bf16[12288,1,128]{0,2,1:T(8,128)(2,1)}, bf16[12288,1,128]{0,2,1:T(8,128)(2,1)}) fusion(bf16[12288,2,128]{0,2,1:T(8,128)(2,1)} %get-tuple-element.211), kind=kLoop, calls=%fused_computation.91 | loop fusion | bytes 12582912 | tf_op jit(solution)/shard_map/split | solution.py:17
  85.3 216.2 %while.18 = (s32[]{:T(128)}, f32[2,1,768]{2,0,1:T(2,128)S(1)}, f32[2,1,768]{2,0,1:T(2,128)}, f32[2,1,768,128]{2,3,0,1:T(8,128)S(1)}, s32[768]{0:T(1024)S(1)}, /*...) while((s32[]{:T(128)}, f32[2,1,768]{2,0,1:T(2,128)S(1)}, ...), condition=%wide.region_5.5_spmd.clone, body=%wide.region_2.4_spmd.clone.sunk | while | flops 311633408 | bytes 25992404 | solution.py:99
  89.0 3.3 fusion.83
  106.4 3.3 fusion.83
  115.4 3.3 fusion.83
  124.4 3.3 fusion.83
  133.5 3.3 fusion.83
  142.5 3.3 fusion.83
  160.6 3.3 fusion.83
  178.7 3.3 fusion.83
  187.7 3.3 fusion.83
  196.7 3.3 fusion.83
  205.8 3.3 fusion.83
  214.8 3.3 fusion.83
  223.8 3.3 fusion.83
  232.9 3.3 fusion.83
  241.9 3.3 fusion.83
  304.3 7.1 %all-to-all-start = ((bf16[16,48,128]{2,1,0:T(8,128)(2,1)}), bf16[16,48,128]{2,1,0:T(8,128)(2,1)S(1)}, u32[]{:S(2)}, u32[]{:S(2)}) async-start(bf16[16,48,128]{2,1,0:T(8,128)(2,1)} %multiply_convert_fusion.1), calls=%async_computation | async-start | bytes 393216 | tf_op jit(solution)/shard_map/all_to_all | solution.py:119
  312.1 9.3 %all-to-all-done = bf16[16,48,128]{2,1,0:T(8,128)(2,1)S(1)} async-done(((bf16[16,48,128]{2,1,0:T(8,128)(2,1)}), bf16[16,48,128]{2,1,0:T(8,128)(2,1)S(1)}, u32[]{:S(2)}, u32[]{:S(2)}) %all-to-all-start) | async-done | bytes 196640 | tf_op jit(solution)/shard_map/all_to_all | solution.py:119
  321.3 5.1 multiply_reduce_fusion.1
  329.3 16.7 %all_to_all.26 = bf16[16,2,4,2048]{3,2,1,0:T(4,128)(2,1)} all-to-all(bf16[16,2,4,2048]{3,2,1,0:T(4,128)(2,1)S(1)} %reshape.361), channel_id=1, replica_groups=mesh['sp'=16,'tp_0'=8,'tp_1'=2] {'sp'}, dimensions={0} | all-to-all | bytes 1048576 | tf_op jit(solution)/shard_map/all_to_all | solution.py:144
  346.2 49.8 %all-gather.6.cloned.1.call-done = bf16[256,2,4,2048]{3,2,1,0:T(4,128)(2,1)} async-done(((bf16[16,2,4,2048]{3,2,1,0:T(4,128)(2,1)}), bf16[256,2,4,2048]{3,2,1,0:T(4,128)(2,1)}) %all-gather.6.cloned.1.call-update) | async-done | bytes 8388624 | tf_op jit(solution)/shard_map/all_gather | solution.py:151
  396.1 11.2 %copy.60 = bf16[256,2,4,2048]{3,0,2,1:T(8,128)(2,1)} copy(bf16[256,2,4,2048]{3,2,1,0:T(4,128)(2,1)} %all-gather.6.cloned.1.call-done) | data formatting | bytes 16777216 | tf_op jit(solution)/shard_map/all_gather | solution.py:151
  407.3 6.7 %fusion.29 = f32[16,16,2,4,128]{4,1,3,0,2:T(8,128)} fusion(bf16[16,16,2,4,2048]{4,1,0,3,2:T(8,128)(2,1)} %bitcast.135, bf16[2,2048,128]{2,1,0:T(8,128)(2,1)S(1)} %copy-done.6), kind=kOutput, calls=%fused_computation.40 | convolution fusion | flops 1073741824 | bytes 10485760 | tf_op jit(solution)/shard_map/tsecd,edf->tsecf/dot_general | solution.py:152
  414.0 13.1 %convolution_convert_fusion = bf16[2,16,16,4,2048]{4,2,3,1,0:T(8,128)(2,1)} fusion(bf16[16,16,2,4,2048]{4,1,0,3,2:T(8,128)(2,1)} %bitcast.136, bf16[2,128,2048]{2,1,0:T(8,128)(2,1)S(1)} %copy-done, bf16[2,2048,128]{2,1,0:T(8,128)(2,1)} %param.28, f32[16,16,2,4,128]{4,1,3,0,2:T(8,128)} %fusion.29), kind=kOutput, calls=%fused_computation.36 | convolution fusion | flops 2153250816 | bytes 19922944 | tf_op jit(solution)/shard_map/tsecf,efd->tsecd/dot_general | solution.py:159
  427.1 8.3 %copy.63 = bf16[8,2,1,16,2,4,2048]{6,3,5,4,2,0,1:T(8,128)(2,1)} copy(bf16[8,2,1,16,2,4,2048]{6,3,5,1,0,4,2:T(8,128)(2,1)} %bitcast.137) | data formatting | bytes 16777216 | tf_op jit(solution)/shard_map/reshape;reshape | solution.py:22
  435.5 20.5 %reduce-scatter.3.cloned.1.call-done = bf16[8,1,16,2,4,2048]{5,2,4,3,1,0:T(8,128)(2,1)} async-done(((bf16[16,1,16,2,4,2048]{5,2,4,3,1,0:T(8,128)(2,1)}), bf16[8,1,16,2,4,2048]{5,2,4,3,1,0:T(8,128)(2,1)}) %reduce-scatter.3.cloned.1.call-update) | async-done | bytes 4194320 | tf_op jit(solution)/shard_map/reduce_scatter | solution.py:26
  456.0 59.0 %reduce-scatter.5.cloned.1.call-done = bf16[1,1,16,2,4,2048]{5,2,4,3,1,0:T(8,128)(2,1)} async-done(((bf16[8,1,16,2,4,2048]{5,2,4,3,1,0:T(8,128)(2,1)}), bf16[1,1,16,2,4,2048]{5,2,4,3,1,0:T(8,128)(2,1)}) %reduce-scatter.5.cloned.1.call-update) | async-done | bytes 524304 | tf_op jit(solution)/shard_map/reduce_scatter | solution.py:26
  517.3 7.3 %all-to-all-start.2 = ((bf16[16,2,4,2048]{3,2,1,0:T(4,128)(2,1)}), bf16[16,2,4,2048]{3,2,1,0:T(4,128)(2,1)S(1)}, u32[]{:S(2)}, u32[]{:S(2)}) async-start(bf16[16,2,4,2048]{3,2,1,0:T(4,128)(2,1)} %copy.64), calls=%async_computation.4 | async-start | bytes 1048576 | tf_op jit(solution)/shard_map/all_to_all | solution.py:167
  524.7 10.0 %all-to-all-done.2 = bf16[16,2,4,2048]{3,2,1,0:T(4,128)(2,1)S(1)} async-done(((bf16[16,2,4,2048]{3,2,1,0:T(4,128)(2,1)}), bf16[16,2,4,2048]{3,2,1,0:T(4,128)(2,1)S(1)}, u32[]{:S(2)}, u32[]{:S(2)}) %all-to-all-start.2) | async-done | bytes 524320 | tf_op jit(solution)/shard_map/all_to_all | solution.py:167
  (310 shorter events, 183.6 us)
Async XLA Ops:
  6.5 407.5 %copy-start = (bf16[2,128,2048]{2,1,0:T(8,128)(2,1)S(1)}, bf16[2,128,2048]{2,1,0:T(8,128)(2,1)}, u32[]{:S(2)}) copy-start(bf16[2,128,2048]{2,1,0:T(8,128)(2,1)} %param.29) | copy-start | bytes 3145732
  6.5 72.4 %all-gather.4.cloned.1.call-start = ((), (), s32[]{:S(2)}) async-start(), calls=%async_computation.5 | async-start | bytes 6684672 | tf_op jit(solution)/shard_map/all_gather | solution.py:16
  78.9 224.3 %copy-start.5 = (f32[128]{0:T(128)S(1)}, f32[128]{0:T(128)}, u32[]{:S(2)}) copy-start(f32[128]{0:T(128)} %param.21) | copy-start | bytes 1540
  78.9 6.2 %copy-start.2 = (bf16[768,1,128]{2,0,1:T(8,128)(2,1)S(1)}, bf16[768,1,128]{2,0,1:T(8,128)(2,1)}, u32[]{:S(2)}) copy-start(bf16[768,1,128]{2,0,1:T(8,128)(2,1)} %get-tuple-element.212) | copy-start | bytes 589828 | tf_op jit(solution)/shard_map/cond
  89.0 3.3 copy-start.1
  106.3 3.3 copy-start.1
  115.4 3.3 copy-start.1
  124.4 3.3 copy-start.1
  133.5 3.3 copy-start.1
  142.5 3.3 copy-start.1
  160.6 3.3 copy-start.1
  169.6 3.3 copy-start.1
  178.6 3.3 copy-start.1
  187.7 3.3 copy-start.1
  196.7 3.3 copy-start.1
  205.7 3.3 copy-start.1
  214.8 3.3 copy-start.1
  223.8 3.3 copy-start.1
  232.8 3.3 copy-start.1
  241.9 3.3 copy-start.1
  250.9 3.3 copy-start.1
  260.0 3.3 copy-start.1
  269.0 3.3 copy-start.1
  278.0 3.3 copy-start.1
  304.3 17.0 %all-to-all-start = ((bf16[16,48,128]{2,1,0:T(8,128)(2,1)}), bf16[16,48,128]{2,1,0:T(8,128)(2,1)S(1)}, u32[]{:S(2)}, u32[]{:S(2)}) async-start(bf16[16,48,128]{2,1,0:T(8,128)(2,1)} %multiply_convert_fusion.1), calls=%async_computation | async-start | bytes 393216 | tf_op jit(solution)/shard_map/all_to_all | solution.py:119
  311.4 84.6 %all-gather.6.cloned.1.call-start = ((), (), s32[]{:S(2)}) async-start(), calls=%async_computation.8 | async-start | bytes 8912896 | tf_op jit(solution)/shard_map/all_gather | solution.py:151
  312.0 14.4 %copy-start.3 = (f32[2048]{0:T(1024)S(1)}, f32[2048]{0:T(1024)}, u32[]{:S(2)}) copy-start(f32[2048]{0:T(1024)} %param.24) | copy-start | bytes 24580
  346.0 61.3 %copy-start.6 = (bf16[2,2048,128]{2,1,0:T(8,128)(2,1)S(1)}, bf16[2,2048,128]{2,1,0:T(8,128)(2,1)}, u32[]{:S(2)}) copy-start(bf16[2,2048,128]{2,1,0:T(8,128)(2,1)} %param.27) | copy-start | bytes 3145732
  346.0 110.0 %reduce-scatter.3.cloned.1.call-start = ((), (), s32[]{:S(2)}) async-start(), calls=%async_computation.6 | async-start | bytes 12582912 | tf_op jit(solution)/shard_map/reduce_scatter | solution.py:26
  435.4 79.6 %reduce-scatter.5.cloned.1.call-start = ((), (), s32[]{:S(2)}) async-start(), calls=%async_computation.7 | async-start | bytes 4718592 | tf_op jit(solution)/shard_map/reduce_scatter | solution.py:26
  456.0 68.6 %copy-start.4 = (f32[48,2]{0,1:T(2,128)S(1)}, f32[48,2]{0,1:T(2,128)}, u32[]{:S(2)}) copy-start(f32[48,2]{0,1:T(2,128)} %param.26) | copy-start | bytes 1156
  517.3 17.4 %all-to-all-start.2 = ((bf16[16,2,4,2048]{3,2,1,0:T(4,128)(2,1)}), bf16[16,2,4,2048]{3,2,1,0:T(4,128)(2,1)S(1)}, u32[]{:S(2)}, u32[]{:S(2)}) async-start(bf16[16,2,4,2048]{3,2,1,0:T(4,128)(2,1)} %copy.64), calls=%async_computation.4 | async-start | bytes 1048576 | tf_op jit(solution)/shard_map/all_to_all | solution.py:167
  (4 other events, 13.2 us)
Sparse Core Ops, SparseCore 0:
  9.8 69.0 all-gather.3
  346.1 49.9 all-gather.5
  435.6 20.3 reduce-scatter.2
  458.4 56.5 reduce-scatter.4
where the time goes:
time: 547 us; the launch traced here: 544 us
  waiting for transfers between devices  214 us (39%)
  matrix products  162 us (30%)
  other arithmetic  61.1 us (11%)
  local copies, waits for them, and re-layouts  59.7 us (11%)
  blocking collectives  16.7 us (3%)
  starting transfers between devices  14.7 us (3%)
  between operations  14.6 us (3%)
    reduce_scatter x2, waiting for transfers between devices, sum_in_order(): parts = lax.psum_scatter(parts, axes[k], scatter_dimension=0, tiled=True)  79.5 us
    dot_general x24, matrix products, block_step(): jnp.einsum('chqk,khv->chqv', weights.astype(jnp.bfloat16), value_block, p...  78.8 us
    all_gather x1, waiting for transfers between devices, side_by_side(): whole = lax.all_gather(both, axis, axis=dim, tiled=True)  65.7 us
    dot_general x24, matrix products, block_step(): jnp.einsum('qhcd,khcd->chqk', split_queries, key_block, preferred_element...  58.6 us
    all_gather x1, waiting for transfers between devices, shards(): piece_rows = lax.all_gather(arrived[None], TP, axis=0, tiled=True)  49.8 us
    add x24, other arithmetic, block_step(): totals = totals * decay + jnp.sum(weights, axis=3)  30.7 us
    dynamic_slice x24, local copies, waits for them, and re-layouts, block_step(): lax.dynamic_slice_in_dim(key_piece, offset, width_rows, 0)  21.9 us
    reduce_sum x24, other arithmetic, block_step(): totals = totals * decay + jnp.sum(weights, axis=3)  17.8 us
  transfers between devices with their start and end apart: 6, of which 6 were waited for; matrix products, arithmetic and copies ran while one was open for 1% of the time, Pallas kernels for 0%

commit v1 on v0

v1 whole, which is shorter than its diff:
```python
import functools

import jax
import jax.numpy as jnp
from jax import lax
from jax.experimental import pallas as pl
from jax.experimental.pallas import tpu as pltpu
from jax.sharding import PartitionSpec as P

MESH = pl.DeviceIdType.MESH
SIDE = 4
N_SP = 16
N_TP = 16
ROWS = 48
SPAN = N_TP * ROWS
HALF = SPAN // 2
GROUP = 2 * ROWS
TILE_GROUPS = 4
TILE = TILE_GROUPS * GROUP
LANES = 128
HD = 64
DEPTH = 2048
EXPERTS = 32
CAP = 4
SLOTS = EXPERTS * CAP
COLS = 512
NEG = -1e30

ORDER = [
    (0, 0), (-1, 0), (1, 0), (0, -1), (0, 1), (2, 0), (-1, -1), (-1, 1),
    (1, -1), (1, 1), (2, -1), (2, 1), (0, 2), (-1, 2), (1, 2), (2, 2),
]
PLACE = {0: 0, -1: 1, 1: 2, 2: 3}


def pick(index, values):
    out = jnp.int32(values[0])
    for k, value in enumerate(values):
        out = jnp.where(index == k, jnp.int32(value), out)
    return out


def mod(value, size):
    return lax.rem(value + size, size)


def attend_kernel(
    q_hbm, kv_hbm, w_hbm, lam_ref, gain_ref, select_ref, residual_ref, norm_gain_ref,
    updated_ref, slots_ref,
    q_own, q_land, qs, kvb, acc, top, own_heads, heads, w_vmem,
    local_sem, q_send, q_recv, kv_send, kv_recv, head_send, head_recv,
):
    sp = lax.axis_index("sp")
    tp = lax.axis_index("tp")
    x, y = lax.rem(sp, SIDE), sp // SIDE

    barrier = pltpu.get_barrier_semaphore()
    load_w = pltpu.make_async_copy(w_hbm, w_vmem, local_sem.at[0])
    load_w.start()
    load_kv = pltpu.make_async_copy(kv_hbm, kvb.at[sp], local_sem.at[1])
    load_kv.start()
    load_q = pltpu.make_async_copy(q_hbm, q_own, local_sem.at[2])
    load_q.start()

    def greet_plane(d, carry):
        pl.semaphore_signal(
            barrier, inc=1, device_id=(lax.rem(sp + d, N_SP), tp), device_id_type=MESH
        )
        return carry

    lax.fori_loop(1, N_SP, greet_plane, 0)

    def greet_sources(h, carry):
        @pl.when(jnp.logical_or(tp != sp, h != tp))
        def _():
            pl.semaphore_signal(barrier, inc=1, device_id=(tp, h), device_id_type=MESH)

        return carry

    lax.fori_loop(0, N_TP, greet_sources, 0)
    pl.semaphore_wait(
        barrier, N_SP - 1 + N_TP - jnp.where(sp == tp, jnp.int32(1), jnp.int32(0))
    )

    load_q.wait()

    def q_copy(d):
        other = lax.rem(sp + d, N_SP)
        return pltpu.make_async_remote_copy(
            src_ref=q_own.at[other], dst_ref=q_land.at[sp],
            send_sem=q_send.at[d], recv_sem=q_recv.at[d],
            device_id=(other, tp), device_id_type=MESH,
        )

    def send_q(d, carry):
        q_copy(d).start()
        return carry

    lax.fori_loop(1, N_SP, send_q, 0)
    load_kv.wait()

    def block_of(half, du, dv):
        dx, dy = (du, dv) if half == 0 else (dv, du)
        return mod(y + dy, SIDE) * SIDE + mod(x + dx, SIDE)

    def kv_copy(half, index, block, part, du, dv):
        ref = kvb.at[block, half] if part is None else kvb.at[block, half, part]
        return pltpu.make_async_remote_copy(
            src_ref=ref, dst_ref=ref,
            send_sem=kv_send.at[half, index], recv_sem=kv_recv.at[half, index],
            device_id=(block_of(half, du, dv), tp), device_id_type=MESH,
        )

    def send(half, index, rel, part, du, dv):
        kv_copy(half, index, block_of(half, *rel), part, du, dv).start()

    def arrived(half, index, rel, part):
        kv_copy(half, index, block_of(half, *rel), part, 1, 0).wait_recv()

    for half in range(2):
        send(half, 0, (0, 0), None, 1, 0)
        send(half, 1, (0, 0), None, -1, 0)
        send(half, 4, (0, 0), None, 0, 1)
        send(half, 8, (0, 0), None, 0, -1)

    for own in range(N_SP):
        @pl.when(sp == own)
        def _():
            q_land[own] = q_own[own]

    lane = lax.broadcasted_iota(jnp.int32, (ROWS, LANES), 1)

    def wait_q(d, carry):
        q_copy(d).wait_recv()
        return carry

    lax.fori_loop(1, N_SP, wait_q, 0)

    def pack_q(g, carry):
        rows = q_land[g].astype(jnp.float32) * (HD**-0.5)
        qs[g, 0:ROWS] = jnp.where(lane < HD, rows, 0.0).astype(jnp.bfloat16)
        qs[g, ROWS:GROUP] = jnp.where(lane >= HD, rows, 0.0).astype(jnp.bfloat16)
        return carry

    lax.fori_loop(0, N_SP, pack_q, 0)
    acc[...] = jnp.zeros_like(acc)
    top[...] = jnp.full_like(top, NEG)

    row = lax.broadcasted_iota(jnp.int32, (TILE_GROUPS, GROUP, HALF), 1)
    row = jnp.where(row >= ROWS, row - ROWS, row)
    offset = (
        lax.broadcasted_iota(jnp.int32, (TILE_GROUPS, GROUP, HALF), 0) * SPAN
        + row
        - lax.broadcasted_iota(jnp.int32, (TILE_GROUPS, GROUP, HALF), 2)
    ).reshape(TILE, HALF)

    def tile_step(t, block, half, masked):
        rows = pl.ds(pl.multiple_of(t * TILE, TILE), TILE)
        q_tile = qs[pl.ds(t * TILE_GROUPS, TILE_GROUPS)].reshape(TILE, LANES)
        keys = kvb[block, half, 0]
        values = kvb[block, half, 1]
        scores = lax.dot_general(
            q_tile, keys, (((1,), (1,)), ((), ())), preferred_element_type=jnp.float32
        )
        if masked:
            ahead = block * SPAN + half * HALF - t * (TILE_GROUPS * SPAN) - sp * ROWS
            scores = jnp.where(offset >= ahead, scores, -jnp.inf)
        old_top = top[rows]
        new_top = jnp.maximum(old_top, jnp.max(scores, axis=1, keepdims=True))
        decay = jnp.exp(old_top - new_top)
        weights = jnp.exp(scores - new_top[:, 0:1]).astype(jnp.bfloat16)
        wide = jnp.concatenate([values, jnp.ones_like(values)], axis=1)
        fresh = jnp.dot(weights, wide, preferred_element_type=jnp.float32)
        acc[rows] = acc[rows] * jnp.concatenate([decay, decay], axis=1) + fresh
        top[rows] = new_top

    def use_block(block, half):
        first = block // TILE_GROUPS
        tile_step(first, block, half, True)

        def later(t, carry):
            tile_step(t, block, half, False)
            return carry

        lax.fori_loop(first + 1, N_SP // TILE_GROUPS, later, 0)

    def step(s, carry):
        def on(k, half):
            du, dv = ORDER[k]
            if k == 1:
                arrived(half, 0, (-1, 0), None)
                send(half, 2, (-1, 0), 0, 1, 0)
                send(half, 5, (-1, 0), None, 0, 1)
                send(half, 9, (-1, 0), None, 0, -1)
            elif k == 2:
                arrived(half, 1, (1, 0), None)
                send(half, 3, (1, 0), 1, -1, 0)
                send(half, 6, (1, 0), None, 0, 1)
                send(half, 10, (1, 0), None, 0, -1)
            elif k == 5:
                arrived(half, 2, (2, 0), 0)
                arrived(half, 3, (2, 0), 1)
                send(half, 7, (2, 0), None, 0, 1)
                send(half, 11, (2, 0), None, 0, -1)
            elif dv == -1:
                place = PLACE[du]
                arrived(half, 4 + place, (du, dv), None)
                send(half, 12 + place, (du, dv), 0, 0, 1)
            elif dv == 1:
                place = PLACE[du]
                arrived(half, 8 + place, (du, dv), None)
                send(half, 16 + place, (du, dv), 1, 0, -1)
            elif dv == 2:
                place = PLACE[du]
                arrived(half, 12 + place, (du, dv), 0)
                arrived(half, 16 + place, (du, dv), 1)

        for k in range(1, len(ORDER)):
            @pl.when(s == k)
            def _():
                for half in range(2):
                    on(k, half)

        du = pick(s, [o[0] for o in ORDER])
        dv = pick(s, [o[1] for o in ORDER])

        def one_half(half, carry):
            dx = jnp.where(half == 0, du, dv)
            dy = jnp.where(half == 0, dv, du)
            block = mod(y + dy, SIDE) * SIDE + mod(x + dx, SIDE)
            use_block(block, half)
            return carry

        return lax.fori_loop(0, 2, one_half, carry)

    lax.fori_loop(0, len(ORDER), step, 0)

    lam = lam_ref[0, 0]

    def finish(g, carry):
        part = acc[pl.ds(pl.multiple_of(g * GROUP, GROUP), GROUP)]
        ratio = part[:, 0:LANES] / part[:, LANES : 2 * LANES]
        mixed = ratio[0:ROWS] - lam * ratio[ROWS:GROUP]
        square = jnp.mean(mixed * mixed, axis=1, keepdims=True)
        own_heads[g] = (mixed * lax.rsqrt(square + 1e-06) * gain_ref[...]).astype(
            jnp.bfloat16
        )
        return carry

    lax.fori_loop(0, N_SP, finish, 0)

    def head_copy(g, h):
        return pltpu.make_async_remote_copy(
            src_ref=own_heads.at[g],
            dst_ref=heads.at[:, pl.ds(pl.multiple_of(tp * LANES, LANES), LANES)],
            send_sem=head_send.at[g], recv_sem=head_recv.at[h],
            device_id=(g, sp), device_id_type=MESH,
        )

    def push_head(g, carry):
        @pl.when(jnp.logical_or(g != sp, sp != tp))
        def _():
            head_copy(g, tp).start()

        return carry

    lax.fori_loop(0, N_SP, push_head, 0)

    for own in range(N_SP):
        @pl.when(jnp.logical_and(sp == own, tp == own))
        def _():
            heads[:, own * LANES : (own + 1) * LANES] = own_heads[own]

    load_w.wait()

    def wait_head(h, carry):
        @pl.when(jnp.logical_or(h != tp, sp != tp))
        def _():
            head_copy(0, h).wait_recv()

        return carry

    lax.fori_loop(0, N_TP, wait_head, 0)

    attended = heads[...]
    squares = jnp.zeros((ROWS, 1), jnp.float32)
    wide = []
    for n in range(DEPTH // COLS):
        cols = slice(n * COLS, (n + 1) * COLS)
        projected = jnp.dot(attended, w_vmem[:, cols], preferred_element_type=jnp.float32)
        updated = (residual_ref[:, cols].astype(jnp.float32) + projected).astype(jnp.bfloat16)
        updated_ref[:, cols] = updated
        back = updated.astype(jnp.float32)
        squares = squares + jnp.sum(back * back, axis=1, keepdims=True)
        wide.append(back)
    scale = lax.rsqrt(squares / DEPTH + 1e-06)
    for n in range(DEPTH // COLS):
        cols = slice(n * COLS, (n + 1) * COLS)
        normed = (wide[n] * scale * norm_gain_ref[:, cols]).astype(jnp.bfloat16)
        slots_ref[:, cols] = jnp.dot(
            select_ref[...], normed, preferred_element_type=jnp.float32
        ).astype(jnp.bfloat16)

    def drain_q(d, carry):
        q_copy(d).wait_send()
        return carry

    lax.fori_loop(1, N_SP, drain_q, 0)

    def drain_heads(g, carry):
        @pl.when(jnp.logical_or(g != sp, sp != tp))
        def _():
            head_copy(g, tp).wait_send()

        return carry

    lax.fori_loop(0, N_SP, drain_heads, 0)
    for half in range(2):
        for index in range(20):
            part = None if index in (0, 1) or 4 <= index < 12 else 0
            kv_copy(half, index, sp, part, 1, 0).wait_send()


def attend(q, kv, w, lam, gain, select, residual, norm_gain):
    anywhere = pl.BlockSpec(memory_space=pl.ANY)
    vmem = pl.BlockSpec(memory_space=pltpu.VMEM)
    smem = pl.BlockSpec(memory_space=pltpu.SMEM)
    dma = pltpu.SemaphoreType.DMA
    return pl.pallas_call(
        attend_kernel,
        out_shape=(
            jax.ShapeDtypeStruct((ROWS, DEPTH), jnp.bfloat16),
            jax.ShapeDtypeStruct((SLOTS, DEPTH), jnp.bfloat16),
        ),
        in_specs=[anywhere, anywhere, anywhere, smem, vmem, vmem, vmem, vmem],
        out_specs=(vmem, vmem),
        scratch_shapes=[
            pltpu.VMEM((N_SP, ROWS, LANES), jnp.bfloat16),
            pltpu.VMEM((N_SP, ROWS, LANES), jnp.bfloat16),
            pltpu.VMEM((N_SP, GROUP, LANES), jnp.bfloat16),
            pltpu.VMEM((N_SP, 2, 2, HALF, LANES), jnp.bfloat16),
            pltpu.VMEM((N_SP * GROUP, 2 * LANES), jnp.float32),
            pltpu.VMEM((N_SP * GROUP, LANES), jnp.float32),
            pltpu.VMEM((N_SP, ROWS, LANES), jnp.bfloat16),
            pltpu.VMEM((ROWS, DEPTH), jnp.bfloat16),
            pltpu.VMEM((DEPTH, DEPTH), jnp.bfloat16),
            dma((3,)),
            dma((N_SP,)),
            dma((N_SP,)),
            dma((2, 20)),
            dma((2, 20)),
            dma((N_SP,)),
            dma((N_TP,)),
        ],
        compiler_params=pltpu.CompilerParams(
            collective_id=0, has_side_effects=True, vmem_limit_bytes=56 * 1024 * 1024
        ),
        name="attend",
    )(q, kv, w, lam, gain, select, residual, norm_gain)


def side_sum(parts, axes, turns):
    shape = [lax.axis_size(a) for a in axes]
    parts = parts.reshape(*shape, *parts.shape[1:])
    parts = parts.transpose(*turns, *range(len(axes), parts.ndim))
    parts = parts.reshape(-1, *parts.shape[len(axes) :])
    for k in turns:
        parts = lax.psum_scatter(parts, axes[k], scatter_dimension=0, tiled=True)
    return parts[0]


def shards(
    queries, key_pairs, head_values, lambdas, head_gain, out_weight, residual, norm_gain,
    expert_ids, route_weights, gate_weight, up_weight, down_weight,
):
    q = queries.reshape(N_SP, ROWS, LANES)
    kv = jnp.stack(
        [key_pairs.reshape(2, HALF, LANES), head_values.reshape(2, HALF, LANES)], axis=1
    )
    flat_ids = expert_ids.reshape(-1)
    routes = flat_ids.shape[0]
    same = flat_ids[:, None] == flat_ids[None, :]
    earlier = jnp.arange(routes)[:, None] > jnp.arange(routes)[None, :]
    ranking = jnp.sum((same & earlier).astype(jnp.int32), axis=1)
    slots = (flat_ids * CAP + ranking).reshape(ROWS, 2)
    hit = slots[:, :, None] == jnp.arange(SLOTS, dtype=jnp.int32)[None, None, :]
    select = jnp.any(hit, axis=1).T.astype(jnp.bfloat16)
    updated, outgoing = attend(
        q, kv, out_weight, lambdas.reshape(1, 1), head_gain.reshape(1, LANES), select,
        residual, norm_gain.reshape(1, DEPTH),
    )
    arrived = lax.all_to_all(
        outgoing.reshape(N_SP, 2, CAP, DEPTH), "sp", split_axis=0, concat_axis=0, tiled=True
    )
    piece_rows = lax.all_gather(arrived[None], "tp", axis=0, tiled=True)
    gate_part = jnp.einsum(
        "tsecd,edf->tsecf", piece_rows, gate_weight, preferred_element_type=jnp.float32
    )
    up_part = jnp.einsum(
        "tsecd,edf->tsecf", piece_rows, up_weight, preferred_element_type=jnp.float32
    )
    inner_rows = (jax.nn.silu(gate_part) * up_part).astype(jnp.bfloat16)
    partial_value = jnp.einsum(
        "tsecf,efd->tsecd", inner_rows, down_weight, preferred_element_type=jnp.float32
    )
    reduced = lax.psum_scatter(
        partial_value.astype(jnp.bfloat16), "tp", scatter_dimension=0, tiled=True
    )
    returned = lax.all_to_all(reduced[0], "sp", split_axis=0, concat_axis=0, tiled=True)
    weight = jnp.sum(jnp.where(hit, route_weights[:, :, None], 0.0), axis=1)
    moe_sum = jnp.dot(
        weight, returned.reshape(SLOTS, DEPTH).astype(jnp.float32), precision=lax.Precision.HIGHEST
    )
    return (updated.astype(jnp.float32) + moe_sum).astype(jnp.bfloat16)


def solution(mesh):
    in_specs = (
        P("sp", "tp", None),
        P("sp", "tp", None),
        P("sp", "tp", None),
        P("tp"),
        P(),
        P(),
        P(("sp", "tp"), None),
        P(),
        P(("sp", "tp"), None),
        P(("sp", "tp"), None),
        P("sp", None, "tp"),
        P("sp", None, "tp"),
        P("sp", "tp", None),
    )
    return jax.shard_map(
        shards, mesh=mesh, in_specs=in_specs, out_specs=P(("sp", "tp"), None), check_vma=False
    )
```

time: 547 us -> 372 us (0.68)
  matrix products: 162 us -> 20.7 us
  Pallas kernels: 0 us -> 104 us
  other arithmetic: 61.1 us -> 2.86 us
  local copies, waits for them, and re-layouts: 59.7 us -> 8.6 us
  waiting for transfers between devices: 214 us -> 195 us
  starting transfers between devices: 14.7 us -> 7.32 us
    dot_general x49 -> x1, matrix products: 142 us -> 1.03 us  [shards(): jnp.dot(weight, returned.reshape(SLOTS, DEPTH).astype(jnp.float32), preci...]
    unnamed x4 -> x3, waiting for transfers between devices: 0.07 us -> 132 us
    pallas_call x0 -> x1, Pallas kernels: none -> 104 us  [attend(): pl.pallas_call(attend_kernel, out_shape=(jax.ShapeDtypeStruct((ROWS, DEPT...]
    reduce_scatter x2 -> x0, waiting for transfers between devices: 79.5 us -> none  [sum_in_order(): parts = lax.psum_scatter(parts, axes[k], scatter_dimension=0, tiled=True)]
    all_gather x2 -> x1, waiting for transfers between devices: 116 us -> 53.6 us  [shards(): piece_rows = lax.all_gather(arrived[None], 'tp', axis=0, tiled=True)]
    add x49 -> x1, other arithmetic: 30.8 us -> 0.7 us  [shards(): slots = (flat_ids * CAP + ranking).reshape(ROWS, 2)]
    dynamic_slice x24 -> x0, local copies, waits for them, and re-layouts: 21.9 us -> none  [block_step(): lax.dynamic_slice_in_dim(key_piece, offset, width_rows, 0)]
    reduce_sum x27 -> x2, other arithmetic: 19.5 us -> 0.26 us  [the longest x1 0.18 us: shards(): ranking = jnp.sum((same & earlier).astype(jnp.int32), axis=1)]
  transfers between devices with their start and end apart: 6 -> 3, of which waited for: 6 -> 3; matrix products, arithmetic and copies ran while one was open for 1% -> 0% of each run, Pallas kernels for 0% -> 0%
where the time goes in v1:
time: 372 us
  waiting for transfers between devices  195 us (52%)
  Pallas kernels  104 us (28%)
  matrix products  20.7 us (6%)
  blocking collectives  19.1 us (5%)
  between operations  14.1 us (4%)
  local copies, waits for them, and re-layouts  8.6 us (2%)
  starting transfers between devices  7.32 us (2%)
    unnamed x3, waiting for transfers between devices  132 us
    pallas_call x1, Pallas kernels, attend(): pl.pallas_call(attend_kernel, out_shape=(jax.ShapeDtypeStruct((ROWS, DEPT...  104 us
    all_gather x1, waiting for transfers between devices, shards(): piece_rows = lax.all_gather(arrived[None], 'tp', axis=0, tiled=True)  53.6 us
    all_to_all x1, blocking collectives, shards(): lax.all_to_all(outgoing.reshape(N_SP, 2, CAP, DEPTH), 'sp', split_axis=0,...  19.1 us
    dot_general x1, matrix products, shards(): jnp.einsum('tsecf,efd->tsecd', inner_rows, down_weight, preferred_element...  13 us
    all_to_all x1, waiting for transfers between devices, shards(): lax.all_to_all(reduced[0], 'sp', split_axis=0, concat_axis=0, tiled=True)  8.66 us
  transfers between devices with their start and end apart: 3, of which 3 were waited for; matrix products, arithmetic and copies ran while one was open for 0% of the time, Pallas kernels for 0%

profile of v1, /device:TPU:2, one launch (start us, length us, event | category | flops | bytes accessed | tf_op | source)
XLA Modules:
  0.0 371.6 jit_solution(17322826591252245468)
XLA Ops:
  6.5 0.0 copy-start
  6.5 0.0 all-gather.3.cloned.1.call-start
  6.5 0.9 copy.42
  7.5 0.1 eq.28
  7.6 0.2 convert_reduce_fusion
  7.8 0.1 reduce_sum.21
  7.9 0.1 copy.43
  8.0 0.7 multiply_add_fusion
  8.7 0.1 fusion.29
  8.8 0.7 copy.44
  10.1 1.8 pad_maximum_fusion.kv_hbm
  12.0 104.3 %attend.1 = (bf16[48,2048]{1,0:T(8,128)(2,1)}, bf16[128,2048]{1,0:T(8,128)(2,1)}) custom-call(bf16[16,48,128]{2,1,0:T(8,128)(2,1)} %bitcast.52, bf16[2,2,384,128]{3,2,1,0:T(8,128)(2,1)} %pad_maximum_fusion.kv_hbm, bf16[2048,2048]{1,0:T(8,128)(2,1)} %w_hbm.1, f32[1,1]{1,0:T(1,128)} %bitcast.49.lam_ref, f32[1,128]{1,0:T(1,128)} %bitcast.55, ...), custom_call_target="tpu_custom_call" | custom-call | tf_op jit(solution)/shard_map/attend/pallas_call | solution.py:329
  116.3 1.2 reshape.32
  117.5 19.1 %all_to_all.10 = bf16[16,2,4,2048]{3,2,1,0:T(4,128)(2,1)S(1)} all-to-all(bf16[16,2,4,2048]{3,2,1,0:T(4,128)(2,1)S(1)} %reshape.32), channel_id=1, replica_groups=mesh['sp'=16,'tp'=16] {'sp'}, dimensions={0} | all-to-all | bytes 1048576 | tf_op jit(solution)/shard_map/all_to_all | solution.py:392
  136.6 1.1 copy.45
  137.7 0.0 all-gather.3.cloned.1.call-update
  137.8 0.0 all-reduce.3.cloned.1.call-start
  137.8 53.6 %all-gather.3.cloned.1.call-done = bf16[256,2,4,2048]{3,0,2,1:T(8,128)(2,1)} async-done(((bf16[16,2,4,2048]{3,0,2,1:T(8,128)(2,1)}), bf16[256,2,4,2048]{3,0,2,1:T(8,128)(2,1)}) %all-gather.3.cloned.1.call-update) | async-done | bytes 8388624 | tf_op jit(solution)/shard_map/all_gather | solution.py:395
  191.4 0.0 copy-done.3
  191.4 6.7 %fusion.5 = f32[16,16,2,4,128]{4,1,3,0,2:T(8,128)} fusion(bf16[16,16,2,4,2048]{4,1,0,3,2:T(8,128)(2,1)} %bitcast.56, bf16[2,2048,128]{2,1,0:T(8,128)(2,1)S(1)} %copy-done.3), kind=kOutput, calls=%fused_computation.7 | convolution fusion | flops 1073741824 | bytes 10485760 | tf_op jit(solution)/shard_map/tsecd,edf->tsecf/dot_general | solution.py:396
  198.1 13.0 %convert_bitcast_fusion = bf16[16,16,2,4,2048]{4,1,3,0,2:T(8,128)(2,1)} fusion(bf16[16,16,2,4,2048]{4,1,0,3,2:T(8,128)(2,1)} %bitcast.57, bf16[2,128,2048]{2,1,0:T(8,128)(2,1)S(1)} %copy-done, bf16[2,2048,128]{2,1,0:T(8,128)(2,1)S(1)} %copy-done.4, f32[16,16,2,4,128]{4,1,3,0,2:T(8,128)} %fusion.5), kind=kOutput, calls=%fused_computation | convolution fusion | flops 2153250816 | bytes 19922944 | tf_op jit(solution)/shard_map/tsecf,efd->tsecd/dot_general | solution.py:403
  211.0 0.0 all-reduce.3.cloned.1.call-update
  211.0 0.6 copy-done.5
  211.7 0.6 dynamic-slice
  212.3 132.4 %all-reduce.3.cloned.1.call-done = bf16[16,16,2,4,2048]{4,1,3,0,2:T(8,128)(2,1)} async-done(((bf16[16,16,2,4,2048]{4,1,3,0,2:T(8,128)(2,1)}), bf16[16,16,2,4,2048]{4,1,3,0,2:T(8,128)(2,1)}) %all-reduce.3.cloned.1.call-update) | async-done | bytes 8388624
  344.6 1.7 dynamic-slice_bitcast_fusion
  346.4 1.2 copy.48
  347.6 7.3 %all-to-all-start.1 = ((bf16[16,2,4,2048]{3,2,1,0:T(4,128)(2,1)}), bf16[16,2,4,2048]{3,2,1,0:T(4,128)(2,1)S(1)}, u32[]{:S(2)}, u32[]{:S(2)}) async-start(bf16[16,2,4,2048]{3,2,1,0:T(4,128)(2,1)} %copy.48), calls=%async_computation.1 | async-start | bytes 1048576 | tf_op jit(solution)/shard_map/all_to_all | solution.py:409
  354.9 0.1 select_reduce_fusion
  355.0 8.7 %all-to-all-done.1 = bf16[16,2,4,2048]{3,2,1,0:T(4,128)(2,1)S(1)} async-done(((bf16[16,2,4,2048]{3,2,1,0:T(4,128)(2,1)}), bf16[16,2,4,2048]{3,2,1,0:T(4,128)(2,1)S(1)}, u32[]{:S(2)}, u32[]{:S(2)}) %all-to-all-start.1) | async-done | bytes 524320 | tf_op jit(solution)/shard_map/all_to_all | solution.py:409
  363.6 0.1 reshape.33
  363.7 1.0 fusion.4
  (10 shorter events, 0.0 us)
Async XLA Ops:
  6.5 191.5 %copy-start = (bf16[2,128,2048]{2,1,0:T(8,128)(2,1)S(1)}, bf16[2,128,2048]{2,1,0:T(8,128)(2,1)}, u32[]{:S(2)}) copy-start(bf16[2,128,2048]{2,1,0:T(8,128)(2,1)} %param.25) | copy-start | bytes 3145732
  6.5 184.8 %copy-start.3 = (bf16[2,2048,128]{2,1,0:T(8,128)(2,1)S(1)}, bf16[2,2048,128]{2,1,0:T(8,128)(2,1)}, u32[]{:S(2)}) copy-start(bf16[2,2048,128]{2,1,0:T(8,128)(2,1)} %param.23) | copy-start | bytes 3145732
  6.5 184.8 %all-gather.3.cloned.1.call-start = ((), (), s32[]{:S(2)}) async-start(), calls=%async_computation.2 | async-start | bytes 8912896 | tf_op jit(solution)/shard_map/all_gather | solution.py:395
  136.6 61.4 %copy-start.4 = (bf16[2,2048,128]{2,1,0:T(8,128)(2,1)S(1)}, bf16[2,2048,128]{2,1,0:T(8,128)(2,1)}, u32[]{:S(2)}) copy-start(bf16[2,2048,128]{2,1,0:T(8,128)(2,1)} %param.24) | copy-start | bytes 3145732
  137.8 206.9 %all-reduce.3.cloned.1.call-start = ((), (), s32[]{:S(2)}) async-start(), calls=%async_computation.3 | async-start | bytes 16777216
  211.0 0.7 copy-start.5
  211.0 143.8 %copy-start.2 = (f32[48,2]{0,1:T(2,128)S(1)}, f32[48,2]{0,1:T(2,128)}, u32[]{:S(2)}) copy-start(f32[48,2]{0,1:T(2,128)} %param.22) | copy-start | bytes 1156
  211.0 152.7 %copy-start.1 = (bf16[48,2048]{1,0:T(8,128)(2,1)S(1)}, bf16[48,2048]{1,0:T(8,128)(2,1)}, u32[]{:S(2)}) copy-start(bf16[48,2048]{1,0:T(8,128)(2,1)} %get-tuple-element.7) | copy-start | bytes 589828
  347.6 16.0 %all-to-all-start.1 = ((bf16[16,2,4,2048]{3,2,1,0:T(4,128)(2,1)}), bf16[16,2,4,2048]{3,2,1,0:T(4,128)(2,1)S(1)}, u32[]{:S(2)}, u32[]{:S(2)}) async-start(bf16[16,2,4,2048]{3,2,1,0:T(4,128)(2,1)} %copy.48), calls=%async_computation.1 | async-start | bytes 1048576 | tf_op jit(solution)/shard_map/all_to_all | solution.py:409
Sparse Core Ops, SparseCore 0:
  137.9 53.4 all-gather.2
  211.2 133.4 all-reduce.2

commit v2 on v1

--- a/solution.py
+++ b/solution.py
@@ -297,9 +297,8 @@
     for n in range(DEPTH // COLS):
         cols = slice(n * COLS, (n + 1) * COLS)
         normed = (wide[n] * scale * norm_gain_ref[:, cols]).astype(jnp.bfloat16)
-        slots_ref[:, cols] = jnp.dot(
-            select_ref[...], normed, preferred_element_type=jnp.float32
-        ).astype(jnp.bfloat16)
+        packed = jnp.dot(select_ref[...], normed, preferred_element_type=jnp.float32)
+        slots_ref[:, :, cols] = packed.reshape(N_SP, 8, COLS).astype(jnp.bfloat16)
 
     def drain_q(d, carry):
         q_copy(d).wait_send()
@@ -330,7 +329,7 @@
         attend_kernel,
         out_shape=(
             jax.ShapeDtypeStruct((ROWS, DEPTH), jnp.bfloat16),
-            jax.ShapeDtypeStruct((SLOTS, DEPTH), jnp.bfloat16),
+            jax.ShapeDtypeStruct((N_SP, 8, DEPTH), jnp.bfloat16),
         ),
         in_specs=[anywhere, anywhere, anywhere, smem, vmem, vmem, vmem, vmem],
         out_specs=(vmem, vmem),
@@ -359,14 +358,338 @@
     )(q, kv, w, lam, gain, select, residual, norm_gain)
 
 
-def side_sum(parts, axes, turns):
-    shape = [lax.axis_size(a) for a in axes]
-    parts = parts.reshape(*shape, *parts.shape[1:])
-    parts = parts.transpose(*turns, *range(len(axes), parts.ndim))
-    parts = parts.reshape(-1, *parts.shape[len(axes) :])
-    for k in turns:
-        parts = lax.psum_scatter(parts, axes[k], scatter_dimension=0, tiled=True)
-    return parts[0]
+RING = 8
+PIECE = 8
+WIDE = 2 * LANES
+MID = DEPTH // 2
+Z_ORDER = [0, -1, 1, -2, 2, -3, 3, 4]
+Z_PLACE = {d: k for k, d in enumerate(Z_ORDER)}
+
+
+def expert_kernel(
+    slots_hbm, gate_hbm, up_hbm, down_hbm, comb_hbm, updated_ref,
+    merged_ref,
+    slots_own, rows, gate_up, down, comb_own, comb, own_part, pair_out, pair_in, out,
+    res, red, sum_out, sum_in,
+    local_sem, slot_send, slot_recv, ring_send, ring_recv, fwd_send, fwd_recv,
+    pair_send, pair_recv, res_send, res_recv, comb_send, comb_recv, sum_send, sum_recv,
+):
+    sp = lax.axis_index("sp")
+    tp = lax.axis_index("tp")
+    z, core = tp // 2, lax.rem(tp, 2)
+
+    barrier = pltpu.get_barrier_semaphore()
+
+    def load(k, src, dst):
+        return pltpu.make_async_copy(src, dst, local_sem.at[k])
+
+    loads = [
+        load(0, slots_hbm, slots_own),
+        load(1, slots_hbm.at[sp], rows.at[tp, sp]),
+        load(2, comb_hbm, comb_own),
+        load(3, comb_hbm, comb.at[z]),
+    ]
+    for e in range(2):
+        loads += [
+            load(4 + e, gate_hbm.at[e], gate_up.at[:, e * LANES : (e + 1) * LANES]),
+            load(6 + e, up_hbm.at[e], gate_up.at[:, (2 + e) * LANES : (3 + e) * LANES]),
+            load(8 + e, down_hbm.at[e], down.at[e * LANES : (e + 1) * LANES]),
+        ]
+    for item in loads:
+        item.start()
+
+    def greet_plane(d, carry):
+        pl.semaphore_signal(
+            barrier, inc=1, device_id=(lax.rem(sp + d, N_SP), tp), device_id_type=MESH
+        )
+        return carry
+
+    lax.fori_loop(1, N_SP, greet_plane, 0)
+
+    def at_z(dz):
+        return (sp, 2 * mod(z + dz, RING) + core)
+
+    def greet_ring(d, carry):
+        pl.semaphore_signal(barrier, inc=1, device_id=at_z(d), device_id_type=MESH)
+        return carry
+
+    lax.fori_loop(1, RING, greet_ring, 0)
+    partner = (sp, 2 * z + (1 - core))
+    pl.semaphore_signal(barrier, inc=1, device_id=partner, device_id_type=MESH)
+    pl.semaphore_wait(barrier, N_SP - 1 + RING - 1 + 1)
+
+    def remote(src, dst, send_sem, recv_sem, device):
+        return pltpu.make_async_remote_copy(
+            src_ref=src, dst_ref=dst, send_sem=send_sem, recv_sem=recv_sem,
+            device_id=device, device_id_type=MESH,
+        )
+
+    def slot_copy(d):
+        other = lax.rem(sp + d, N_SP)
+        return remote(
+            slots_own.at[other], rows.at[tp, sp], slot_send.at[d], slot_recv.at[d], (other, tp)
+        )
+
+    loads[0].wait()
+
+    def send_slot(d, carry):
+        slot_copy(d).start()
+        return carry
+
+    lax.fori_loop(1, N_SP, send_slot, 0)
+    loads[2].wait()
+
+    def comb_copy(d):
+        return remote(comb_own, comb.at[z], comb_send.at[d], comb_recv.at[d], at_z(d))
+
+    def send_comb(d, carry):
+        comb_copy(d).start()
+        return carry
+
+    lax.fori_loop(1, RING, send_comb, 0)
+    for item in loads[1:2] + loads[3:]:
+        item.wait()
+
+    def ring_copy(way, m, dz, piece):
+        ref = rows.at[2 * mod(z + dz, RING) + core, pl.ds(piece * PIECE, PIECE)]
+        return remote(
+            ref, ref, ring_send.at[way, m], ring_recv.at[way, m], at_z(1 if way == 0 else -1)
+        )
+
+    def fwd_copy(j, dz):
+        ref = rows.at[2 * mod(z + dz, RING) + core]
+        return remote(ref, ref, fwd_send.at[j], fwd_recv.at[j], partner)
+
+    def pair_copy(j):
+        return remote(pair_out.at[j], pair_in.at[j], pair_send.at[j], pair_recv.at[j], partner)
+
+    def res_copy(j, d):
+        other = lax.rem(sp + d, N_SP)
+        return remote(
+            out.at[j, other], res.at[j, sp], res_send.at[j, d], res_recv.at[j, d], (other, tp)
+        )
+
+    def ring_event(k):
+        if k == 0:
+            for piece in range(2):
+                def wait_slot(src, carry):
+                    d = mod(sp - src, N_SP)
+
+                    @pl.when(d != 0)
+                    def _():
+                        slot_copy(d).wait_recv()
+
+                    return carry
+
+                lax.fori_loop(piece * PIECE, (piece + 1) * PIECE, wait_slot, 0)
+                for way in range(2):
+                    ring_copy(way, piece, 0, piece).start()
+            fwd_copy(0, 0).start()
+        elif k < 4:
+            for piece in range(2):
+                for way in range(2):
+                    dz = -k if way == 0 else k
+                    ring_copy(way, 2 * (k - 1) + piece, dz, piece).wait_recv()
+                    if k < 3:
+                        ring_copy(way, 2 * k + piece, dz, piece).start()
+                    elif piece == way:
+                        ring_copy(way, 6, dz, piece).start()
+            fwd_copy(2 * k - 1, -k).start()
+            fwd_copy(2 * k, k).start()
+        else:
+            ring_copy(0, 6, 4, 0).wait_recv()
+            ring_copy(1, 6, 4, 1).wait_recv()
+            fwd_copy(7, 4).start()
+
+    row_expert = lax.rem(lax.broadcasted_iota(jnp.int32, (2 * N_SP * CAP, WIDE), 0), 8) // CAP
+    col_expert = lax.broadcasted_iota(jnp.int32, (2 * N_SP * CAP, WIDE), 1) // LANES
+    mine = row_expert == col_expert
+
+    def chunk_part(chunk, dst, j):
+        x = rows[chunk].reshape(2 * N_SP * CAP, DEPTH)
+        gate = jnp.dot(x, gate_up[:, 0:WIDE], preferred_element_type=jnp.float32)
+        up = jnp.dot(x, gate_up[:, WIDE : 2 * WIDE], preferred_element_type=jnp.float32)
+        inner = gate / (1.0 + jnp.exp(-gate)) * up
+        inner = jnp.where(mine, inner, 0.0).astype(jnp.bfloat16)
+        for n in range(DEPTH // COLS):
+            cols = slice(n * COLS, (n + 1) * COLS)
+            piece = jnp.dot(inner, down[:, cols], preferred_element_type=jnp.float32)
+            dst[j, :, :, cols] = piece.reshape(N_SP, 8, COLS).astype(jnp.bfloat16)
+
+    def push_results(j):
+        pair_copy(j).wait_recv()
+        total = own_part[j].astype(jnp.float32) + pair_in[j].astype(jnp.float32)
+        out[j] = total.astype(jnp.bfloat16)
+        res[j, sp] = out[j, sp]
+
+        def push(d, carry):
+            res_copy(j, d).start()
+            return carry
+
+        lax.fori_loop(1, N_SP, push, 0)
+
+    def combine(j):
+        def wait_res(d, carry):
+            res_copy(j, d).wait_recv()
+            return carry
+
+        lax.fori_loop(1, N_SP, wait_res, 0)
+        zj = mod(z + pick(j, Z_ORDER), RING)
+
+        @pl.when(zj != z)
+        def _():
+            comb_copy(mod(z - zj, RING)).wait_recv()
+
+        high, low = comb[zj, :, 0:LANES], comb[zj, :, LANES:WIDE]
+        for n in range(DEPTH // COLS):
+            cols = slice(n * COLS, (n + 1) * COLS)
+            found = res[j, :, :, cols].reshape(SLOTS, COLS)
+            red[j, :, cols] = jnp.dot(
+                high, found, preferred_element_type=jnp.float32
+            ) + jnp.dot(low, found, preferred_element_type=jnp.float32)
+
+    def step(j, carry):
+        for k, at in enumerate((0, 1, 3, 5, 7)):
+            @pl.when(j == at)
+            def _():
+                ring_event(k)
+
+        zj = mod(z + pick(j, Z_ORDER), RING)
+        chunk_part(2 * zj + core, own_part, j)
+        fwd_copy(j, 0).wait_recv()
+        chunk_part(2 * zj + (1 - core), pair_out, j)
+        pair_copy(j).start()
+
+        @pl.when(j >= 1)
+        def _():
+            push_results(j - 1)
+
+        @pl.when(j >= 3)
+        def _():
+            combine(j - 3)
+
+        return carry
+
+    lax.fori_loop(0, RING, step, 0)
+    push_results(RING - 1)
+
+    def late(j, carry):
+        combine(j)
+        return carry
+
+    lax.fori_loop(RING - 3, RING, late, 0)
+
+    def sum_copy(way, r, h):
+        cols = slice(h * MID, (h + 1) * MID)
+        return remote(
+            sum_out.at[way, r, :, cols], sum_in.at[way, r, :, cols],
+            sum_send.at[way, r, h], sum_recv.at[way, r, h], at_z(-1 if way == 0 else 1),
+        )
+
+    def sum_step(way, r, h):
+        cols = slice(h * MID, (h + 1) * MID)
+        d = 4 if r == 0 else (r - 4 if way == 0 else 4 - r)
+        value = red[Z_PLACE[d], :, cols]
+        if r > 1 or (r == 1 and h == way):
+            sum_copy(way, r - 1, h).wait_recv()
+            value = value + sum_in[way, r - 1, :, cols].astype(jnp.float32)
+        sum_out[way, r, :, cols] = value.astype(jnp.bfloat16)
+        sum_copy(way, r, h).start()
+
+    sum_step(0, 0, 0)
+    sum_step(1, 0, 1)
+    for r in range(1, 4):
+        sum_step(0, r, 1)
+        sum_step(1, r, 0)
+        sum_step(0, r, 0)
+        sum_step(1, r, 1)
+    for h in range(2):
+        cols = slice(h * MID, (h + 1) * MID)
+        total = updated_ref[:, cols].astype(jnp.float32) + red[0, :, cols]
+        for way in range(2):
+            sum_copy(way, 3, h).wait_recv()
+            total = total + sum_in[way, 3, :, cols].astype(jnp.float32)
+        merged_ref[:, cols] = total.astype(jnp.bfloat16)
+
+    def drain_plane(d, carry):
+        slot_copy(d).wait_send()
+
+        def drain_res(j, inner):
+            res_copy(j, d).wait_send()
+            return inner
+
+        return lax.fori_loop(0, RING, drain_res, carry)
+
+    lax.fori_loop(1, N_SP, drain_plane, 0)
+
+    def drain_comb(d, carry):
+        comb_copy(d).wait_send()
+        return carry
+
+    lax.fori_loop(1, RING, drain_comb, 0)
+
+    def drain_pair(j, carry):
+        fwd_copy(j, 0).wait_send()
+        pair_copy(j).wait_send()
+        return carry
+
+    lax.fori_loop(0, RING, drain_pair, 0)
+    for way in range(2):
+        for m in range(7):
+            ring_copy(way, m, 0, 0).wait_send()
+        for r in range(4):
+            for h in range(2):
+                if r > 0 or h == way:
+                    sum_copy(way, r, h).wait_send()
+
+
+def experts(slots, gate, up, down, comb, updated):
+    anywhere = pl.BlockSpec(memory_space=pl.ANY)
+    vmem = pl.BlockSpec(memory_space=pltpu.VMEM)
+    dma = pltpu.SemaphoreType.DMA
+    chunk = (N_SP, 8, DEPTH)
+    bf16, f32 = jnp.bfloat16, jnp.float32
+    return pl.pallas_call(
+        expert_kernel,
+        out_shape=jax.ShapeDtypeStruct((ROWS, DEPTH), bf16),
+        in_specs=[anywhere] * 5 + [vmem],
+        out_specs=vmem,
+        scratch_shapes=[
+            pltpu.VMEM(chunk, bf16),
+            pltpu.VMEM((N_TP, *chunk), bf16),
+            pltpu.VMEM((DEPTH, 2 * WIDE), bf16),
+            pltpu.VMEM((WIDE, DEPTH), bf16),
+            pltpu.VMEM((ROWS, WIDE), bf16),
+            pltpu.VMEM((RING, ROWS, WIDE), bf16),
+            pltpu.VMEM((RING, *chunk), bf16),
+            pltpu.VMEM((RING, *chunk), bf16),
+            pltpu.VMEM((RING, *chunk), bf16),
+            pltpu.VMEM((RING, *chunk), bf16),
+            pltpu.VMEM((RING, *chunk), bf16),
+            pltpu.VMEM((RING, ROWS, DEPTH), f32),
+            pltpu.VMEM((2, 4, ROWS, DEPTH), bf16),
+            pltpu.VMEM((2, 4, ROWS, DEPTH), bf16),
+            dma((10,)),
+            dma((N_SP,)),
+            dma((N_SP,)),
+            dma((2, 7)),
+            dma((2, 7)),
+            dma((RING,)),
+            dma((RING,)),
+            dma((RING,)),
+            dma((RING,)),
+            dma((RING, N_SP)),
+            dma((RING, N_SP)),
+            dma((RING,)),
+            dma((RING,)),
+            dma((2, 4, 2)),
+            dma((2, 4, 2)),
+        ],
+        compiler_params=pltpu.CompilerParams(
+            collective_id=1, has_side_effects=True, vmem_limit_bytes=56 * 1024 * 1024
+        ),
+        name="experts",
+    )(slots, gate, up, down, comb, updated)
 
 
 def shards(
@@ -385,33 +708,17 @@
     slots = (flat_ids * CAP + ranking).reshape(ROWS, 2)
     hit = slots[:, :, None] == jnp.arange(SLOTS, dtype=jnp.int32)[None, None, :]
     select = jnp.any(hit, axis=1).T.astype(jnp.bfloat16)
+    weight = jnp.sum(jnp.where(hit, route_weights[:, :, None], 0.0), axis=1)
+    high = weight.astype(jnp.bfloat16)
+    low = (weight - high.astype(jnp.float32)).astype(jnp.bfloat16)
     updated, outgoing = attend(
         q, kv, out_weight, lambdas.reshape(1, 1), head_gain.reshape(1, LANES), select,
         residual, norm_gain.reshape(1, DEPTH),
     )
-    arrived = lax.all_to_all(
-        outgoing.reshape(N_SP, 2, CAP, DEPTH), "sp", split_axis=0, concat_axis=0, tiled=True
+    return experts(
+        outgoing, gate_weight, up_weight, down_weight, jnp.concatenate([high, low], axis=1),
+        updated,
     )
-    piece_rows = lax.all_gather(arrived[None], "tp", axis=0, tiled=True)
-    gate_part = jnp.einsum(
-        "tsecd,edf->tsecf", piece_rows, gate_weight, preferred_element_type=jnp.float32
-    )
-    up_part = jnp.einsum(
-        "tsecd,edf->tsecf", piece_rows, up_weight, preferred_element_type=jnp.float32
-    )
-    inner_rows = (jax.nn.silu(gate_part) * up_part).astype(jnp.bfloat16)
-    partial_value = jnp.einsum(
-        "tsecf,efd->tsecd", inner_rows, down_weight, preferred_element_type=jnp.float32
-    )
-    reduced = lax.psum_scatter(
-        partial_value.astype(jnp.bfloat16), "tp", scatter_dimension=0, tiled=True
-    )
-    returned = lax.all_to_all(reduced[0], "sp", split_axis=0, concat_axis=0, tiled=True)
-    weight = jnp.sum(jnp.where(hit, route_weights[:, :, None], 0.0), axis=1)
-    moe_sum = jnp.dot(
-        weight, returned.reshape(SLOTS, DEPTH).astype(jnp.float32), precision=lax.Precision.HIGHEST
-    )
-    return (updated.astype(jnp.float32) + moe_sum).astype(jnp.bfloat16)
 
 
 def solution(mesh):

time: 372 us -> 221 us (0.59)
  waiting for transfers between devices: 195 us -> 0 us
  Pallas kernels: 104 us -> 212 us
  matrix products: 20.7 us -> 0 us
  blocking collectives: 19.1 us -> 0 us
  between operations: 14.1 us -> 0.73 us
  starting transfers between devices: 7.32 us -> 0 us
  local copies, waits for them, and re-layouts: 8.6 us -> 3.43 us
    unnamed x3 -> x0, waiting for transfers between devices: 132 us -> none
    pallas_call x0 -> x1, Pallas kernels: none -> 108 us  [experts(): pl.pallas_call(expert_kernel, out_shape=jax.ShapeDtypeStruct((ROWS, DEPTH...]
    all_gather x1 -> x0, waiting for transfers between devices: 53.6 us -> none  [shards(): piece_rows = lax.all_gather(arrived[None], 'tp', axis=0, tiled=True)]
    dot_general x3 -> x0, matrix products: 20.7 us -> none  [the longest x1 13 us: shards(): jnp.einsum('tsecf,efd->tsecd', inner_rows, down_weight, preferred_element...]
    all_to_all x1 -> x0, blocking collectives: 19.1 us -> none  [shards(): lax.all_to_all(outgoing.reshape(N_SP, 2, CAP, DEPTH), 'sp', split_axis=0,...]
    all_to_all x1 -> x0, waiting for transfers between devices: 8.66 us -> none  [shards(): lax.all_to_all(reduced[0], 'sp', split_axis=0, concat_axis=0, tiled=True)]
    all_to_all x1 -> x0, starting transfers between devices: 7.27 us -> none  [shards(): lax.all_to_all(reduced[0], 'sp', split_axis=0, concat_axis=0, tiled=True)]
  transfers between devices with their start and end apart: 3 -> 0, of which waited for: 3 -> 0; matrix products, arithmetic and copies ran while one was open for 0% -> 0% of each run, Pallas kernels for 0% -> 0%
where the time goes in v2:
time: 221 us; the launch traced here: 220 us
  Pallas kernels  212 us (96%)
  other arithmetic  3.5 us (2%)
  local copies, waits for them, and re-layouts  3.43 us (2%)
    pallas_call x1, Pallas kernels, experts(): pl.pallas_call(expert_kernel, out_shape=jax.ShapeDtypeStruct((ROWS, DEPTH...  108 us
    pallas_call x1, Pallas kernels, attend(): pl.pallas_call(attend_kernel, out_shape=(jax.ShapeDtypeStruct((ROWS, DEPT...  104 us

profile of v2, /device:TPU:2, one launch (start us, length us, event | category | flops | bytes accessed | tf_op | source)
XLA Modules:
  0.0 219.7 jit_solution(4389053767021705984)
XLA Ops:
  0.0 0.0 copy-start
  0.0 1.8 pad_maximum_fusion.kv_hbm
  2.5 0.8 copy.27
  3.2 0.1 eq.28
  3.4 0.2 convert_reduce_fusion
  3.6 0.1 reduce_sum.21
  3.7 0.1 copy.28
  3.8 0.7 multiply_add_fusion
  4.5 0.1 fusion
  4.6 0.7 copy.29
  5.3 104.2 %attend.1 = (bf16[48,2048]{1,0:T(8,128)(2,1)}, bf16[16,8,2048]{2,1,0:T(8,128)(2,1)}) custom-call(bf16[16,48,128]{2,1,0:T(8,128)(2,1)} %bitcast.10, bf16[2,2,384,128]{3,2,1,0:T(8,128)(2,1)} %pad_maximum_fusion.kv_hbm, bf16[2048,2048]{1,0:T(8,128)(2,1)} %w_hbm.1, f32[1,1]{1,0:T(1,128)} %bitcast.7.lam_ref, f32[1,128]{1,0:T(1,128)} %bitcast.13, ...), custom_call_target="tpu_custom_call" | custom-call | tf_op jit(solution)/shard_map/attend/pallas_call | solution.py:328
  109.5 0.0 copy-done
  109.5 0.1 select_reduce_fusion
  109.6 0.6 pad_maximum_fusion.1.comb_hbm
  110.2 107.9 %experts.1 = bf16[48,2048]{1,0:T(8,128)(2,1)} custom-call(bf16[16,8,2048]{2,1,0:T(8,128)(2,1)} %get-tuple-element.7.slots_hbm, bf16[2,2048,128]{2,1,0:T(8,128)(2,1)} %gate_hbm.1, bf16[2,2048,128]{2,1,0:T(8,128)(2,1)} %up_hbm.1, bf16[2,128,2048]{2,1,0:T(8,128)(2,1)} %down_hbm.1, bf16[48,256]{1,0:T(8,128)(2,1)} %pad_maximum_fusion.1.comb_hbm, ...), custom_call_target="tpu_custom_call" | custom-call | tf_op jit(solution)/shard_map/experts/pallas_call | solution.py:652
  218.1 1.6 copy.32
  (2 shorter events, 0.0 us)
Async XLA Ops:
  0.0 109.5 %copy-start = (f32[48,2]{0,1:T(2,128)S(1)}, f32[48,2]{0,1:T(2,128)}, u32[]{:S(2)}) copy-start(f32[48,2]{0,1:T(2,128)} %param.22) | copy-start | bytes 1156

commit v3 on v2

--- a/solution.py
+++ b/solution.py
@@ -14,10 +14,9 @@
 ROWS = 48
 SPAN = N_TP * ROWS
 HALF = SPAN // 2
-GROUP = 2 * ROWS
-TILE_GROUPS = 4
-TILE = TILE_GROUPS * GROUP
 LANES = 128
+TILES = SPAN // LANES
+ONES = 16
 HD = 64
 DEPTH = 2048
 EXPERTS = 32
@@ -47,7 +46,8 @@
 def attend_kernel(
     q_hbm, kv_hbm, w_hbm, lam_ref, gain_ref, select_ref, residual_ref, norm_gain_ref,
     updated_ref, slots_ref,
-    q_own, q_land, qs, kvb, acc, top, own_heads, heads, w_vmem,
+    q_own, q_land, qs, kvb, acc, top, score_a, score_b, weight_a, weight_b,
+    own_heads, heads, w_vmem,
     local_sem, q_send, q_recv, kv_send, kv_recv, head_send, head_recv,
 ):
     sp = lax.axis_index("sp")
@@ -70,24 +70,33 @@
 
     lax.fori_loop(1, N_SP, greet_plane, 0)
 
+    def owner(i, b):
+        return lax.rem(i + b, N_TP)
+
+    source = mod(tp - sp, N_SP)
+    keeps = owner(sp, sp) == tp
+
     def greet_sources(h, carry):
-        @pl.when(jnp.logical_or(tp != sp, h != tp))
+        @pl.when(jnp.logical_or(jnp.logical_not(keeps), h != tp))
         def _():
-            pl.semaphore_signal(barrier, inc=1, device_id=(tp, h), device_id_type=MESH)
+            pl.semaphore_signal(barrier, inc=1, device_id=(source, h), device_id_type=MESH)
 
         return carry
 
     lax.fori_loop(0, N_TP, greet_sources, 0)
     pl.semaphore_wait(
-        barrier, N_SP - 1 + N_TP - jnp.where(sp == tp, jnp.int32(1), jnp.int32(0))
+        barrier, N_SP - 1 + N_TP - jnp.where(keeps, jnp.int32(1), jnp.int32(0))
     )
 
     load_q.wait()
+
+    def row_block(g):
+        return pl.ds(pl.multiple_of(g * ROWS, ROWS), ROWS)
 
     def q_copy(d):
         other = lax.rem(sp + d, N_SP)
         return pltpu.make_async_remote_copy(
-            src_ref=q_own.at[other], dst_ref=q_land.at[sp],
+            src_ref=q_own.at[owner(other, sp)], dst_ref=q_land.at[row_block(sp)],
             send_sem=q_send.at[d], recv_sem=q_recv.at[d],
             device_id=(other, tp), device_id_type=MESH,
         )
@@ -126,9 +135,7 @@
     for own in range(N_SP):
         @pl.when(sp == own)
         def _():
-            q_land[own] = q_own[own]
-
-    lane = lax.broadcasted_iota(jnp.int32, (ROWS, LANES), 1)
+            q_land[own * ROWS : (own + 1) * ROWS] = q_own[2 * own % N_TP]
 
     def wait_q(d, carry):
         q_copy(d).wait_recv()
@@ -136,53 +143,66 @@
 
     lax.fori_loop(1, N_SP, wait_q, 0)
 
-    def pack_q(g, carry):
-        rows = q_land[g].astype(jnp.float32) * (HD**-0.5)
-        qs[g, 0:ROWS] = jnp.where(lane < HD, rows, 0.0).astype(jnp.bfloat16)
-        qs[g, ROWS:GROUP] = jnp.where(lane >= HD, rows, 0.0).astype(jnp.bfloat16)
-        return carry
-
-    lax.fori_loop(0, N_SP, pack_q, 0)
+    lane = lax.broadcasted_iota(jnp.int32, (LANES, LANES), 1)
+    for i in range(TILES):
+        wide = q_land[i * LANES : (i + 1) * LANES].astype(jnp.float32) * (HD**-0.5)
+        qs[i, 0:LANES] = jnp.where(lane < HD, wide, 0.0).astype(jnp.bfloat16)
+        qs[i, LANES : 2 * LANES] = jnp.where(lane >= HD, wide, 0.0).astype(jnp.bfloat16)
     acc[...] = jnp.zeros_like(acc)
     top[...] = jnp.full_like(top, NEG)
 
-    row = lax.broadcasted_iota(jnp.int32, (TILE_GROUPS, GROUP, HALF), 1)
-    row = jnp.where(row >= ROWS, row - ROWS, row)
-    offset = (
-        lax.broadcasted_iota(jnp.int32, (TILE_GROUPS, GROUP, HALF), 0) * SPAN
-        + row
-        - lax.broadcasted_iota(jnp.int32, (TILE_GROUPS, GROUP, HALF), 2)
-    ).reshape(TILE, HALF)
-
-    def tile_step(t, block, half, masked):
-        rows = pl.ds(pl.multiple_of(t * TILE, TILE), TILE)
-        q_tile = qs[pl.ds(t * TILE_GROUPS, TILE_GROUPS)].reshape(TILE, LANES)
+    score_bufs, weight_bufs = (score_a, score_b), (weight_a, weight_b)
+
+    def tiles_step(first, block, half):
         keys = kvb[block, half, 0]
-        values = kvb[block, half, 1]
-        scores = lax.dot_general(
-            q_tile, keys, (((1,), (1,)), ((), ())), preferred_element_type=jnp.float32
-        )
-        if masked:
-            ahead = block * SPAN + half * HALF - t * (TILE_GROUPS * SPAN) - sp * ROWS
-            scores = jnp.where(offset >= ahead, scores, -jnp.inf)
-        old_top = top[rows]
-        new_top = jnp.maximum(old_top, jnp.max(scores, axis=1, keepdims=True))
-        decay = jnp.exp(old_top - new_top)
-        weights = jnp.exp(scores - new_top[:, 0:1]).astype(jnp.bfloat16)
-        wide = jnp.concatenate([values, jnp.ones_like(values)], axis=1)
-        fresh = jnp.dot(weights, wide, preferred_element_type=jnp.float32)
-        acc[rows] = acc[rows] * jnp.concatenate([decay, decay], axis=1) + fresh
-        top[rows] = new_top
+        wide = jnp.concatenate(
+            [kvb[block, half, 1, k * LANES : (k + 1) * LANES] for k in range(HALF // LANES)],
+            axis=1,
+        )
+        wide = jnp.concatenate([wide, jnp.ones((ONES, HALF), jnp.bfloat16)], axis=0)
+
+        def score(i):
+            scores = lax.dot_general(
+                keys, qs[i], (((1,), (1,)), ((), ())), preferred_element_type=jnp.float32
+            )
+            if i < first + 3:
+                place = lax.broadcasted_iota(jnp.int32, (1, LANES), 1) + i * LANES
+                span = lax.shift_right_logical(place * 1366, 16)
+                last = (
+                    span * (SPAN - ROWS) + place + ((sp + span) & (N_TP - 1)) * ROWS
+                    - block * SPAN - half * HALF
+                )
+                kept = lax.broadcasted_iota(jnp.int32, (HALF, LANES), 0) <= last
+                scores = jnp.where(jnp.concatenate([kept, kept], axis=1), scores, -jnp.inf)
+            score_bufs[i % 2][...] = scores
+            old_top = top[i]
+            new_top = jnp.maximum(old_top, jnp.max(scores, axis=0, keepdims=True))
+            top[i] = new_top
+            return new_top, jnp.exp(old_top - new_top)
+
+        def weigh(i, new_top):
+            weights = jnp.exp(score_bufs[i % 2][...] - new_top)
+            weight_bufs[i % 2][...] = weights.astype(jnp.bfloat16)
+
+        def add_up(i, decay):
+            fresh = jnp.dot(wide, weight_bufs[i % 2][...], preferred_element_type=jnp.float32)
+            acc[i] = acc[i] * decay + fresh
+
+        state = {first: score(first)}
+        for i in range(first, TILES + 1):
+            if i + 1 < TILES:
+                state[i + 1] = score(i + 1)
+            if i < TILES:
+                weigh(i, state[i][0])
+            if i > first:
+                add_up(i - 1, state[i - 1][1])
 
     def use_block(block, half):
-        first = block // TILE_GROUPS
-        tile_step(first, block, half, True)
-
-        def later(t, carry):
-            tile_step(t, block, half, False)
-            return carry
-
-        lax.fori_loop(first + 1, N_SP // TILE_GROUPS, later, 0)
+        first = block * ROWS // LANES // 2
+        for k in range(TILES // 2):
+            @pl.when(first == k)
+            def _():
+                tiles_step(2 * k, block, half)
 
     def step(s, carry):
         def on(k, half):
@@ -237,28 +257,23 @@
 
     lam = lam_ref[0, 0]
 
-    def finish(g, carry):
-        part = acc[pl.ds(pl.multiple_of(g * GROUP, GROUP), GROUP)]
-        ratio = part[:, 0:LANES] / part[:, LANES : 2 * LANES]
-        mixed = ratio[0:ROWS] - lam * ratio[ROWS:GROUP]
-        square = jnp.mean(mixed * mixed, axis=1, keepdims=True)
-        own_heads[g] = (mixed * lax.rsqrt(square + 1e-06) * gain_ref[...]).astype(
-            jnp.bfloat16
-        )
-        return carry
-
-    lax.fori_loop(0, N_SP, finish, 0)
+    for i in range(TILES):
+        ratio = acc[i, 0:LANES] / acc[i, LANES : LANES + 1]
+        mixed = ratio[:, 0:LANES] - lam * ratio[:, LANES : 2 * LANES]
+        square = jnp.mean(mixed * mixed, axis=0, keepdims=True)
+        done = (mixed * lax.rsqrt(square + 1e-06)).T * gain_ref[...]
+        own_heads[i * LANES : (i + 1) * LANES] = done.astype(jnp.bfloat16)
 
     def head_copy(g, h):
         return pltpu.make_async_remote_copy(
-            src_ref=own_heads.at[g],
+            src_ref=own_heads.at[row_block(g)],
             dst_ref=heads.at[:, pl.ds(pl.multiple_of(tp * LANES, LANES), LANES)],
             send_sem=head_send.at[g], recv_sem=head_recv.at[h],
-            device_id=(g, sp), device_id_type=MESH,
+            device_id=(g, owner(sp, g)), device_id_type=MESH,
         )
 
     def push_head(g, carry):
-        @pl.when(jnp.logical_or(g != sp, sp != tp))
+        @pl.when(jnp.logical_or(g != sp, jnp.logical_not(keeps)))
         def _():
             head_copy(g, tp).start()
 
@@ -267,14 +282,15 @@
     lax.fori_loop(0, N_SP, push_head, 0)
 
     for own in range(N_SP):
-        @pl.when(jnp.logical_and(sp == own, tp == own))
+        @pl.when(jnp.logical_and(sp == own, keeps))
         def _():
-            heads[:, own * LANES : (own + 1) * LANES] = own_heads[own]
+            at = 2 * own % N_TP * LANES
+            heads[:, at : at + LANES] = own_heads[own * ROWS : (own + 1) * ROWS]
 
     load_w.wait()
 
     def wait_head(h, carry):
-        @pl.when(jnp.logical_or(h != tp, sp != tp))
+        @pl.when(jnp.logical_or(h != tp, jnp.logical_not(keeps)))
         def _():
             head_copy(0, h).wait_recv()
 
@@ -307,7 +323,7 @@
     lax.fori_loop(1, N_SP, drain_q, 0)
 
     def drain_heads(g, carry):
-        @pl.when(jnp.logical_or(g != sp, sp != tp))
+        @pl.when(jnp.logical_or(g != sp, jnp.logical_not(keeps)))
         def _():
             head_copy(g, tp).wait_send()
 
@@ -335,12 +351,16 @@
         out_specs=(vmem, vmem),
         scratch_shapes=[
             pltpu.VMEM((N_SP, ROWS, LANES), jnp.bfloat16),
-            pltpu.VMEM((N_SP, ROWS, LANES), jnp.bfloat16),
-            pltpu.VMEM((N_SP, GROUP, LANES), jnp.bfloat16),
+            pltpu.VMEM((SPAN, LANES), jnp.bfloat16),
+            pltpu.VMEM((TILES, 2 * LANES, LANES), jnp.bfloat16),
             pltpu.VMEM((N_SP, 2, 2, HALF, LANES), jnp.bfloat16),
-            pltpu.VMEM((N_SP * GROUP, 2 * LANES), jnp.float32),
-            pltpu.VMEM((N_SP * GROUP, LANES), jnp.float32),
-            pltpu.VMEM((N_SP, ROWS, LANES), jnp.bfloat16),
+            pltpu.VMEM((TILES, LANES + ONES, 2 * LANES), jnp.float32),
+            pltpu.VMEM((TILES, 1, 2 * LANES), jnp.float32),
+            pltpu.VMEM((HALF, 2 * LANES), jnp.float32),
+            pltpu.VMEM((HALF, 2 * LANES), jnp.float32),
+            pltpu.VMEM((HALF, 2 * LANES), jnp.bfloat16),
+            pltpu.VMEM((HALF, 2 * LANES), jnp.bfloat16),
+            pltpu.VMEM((SPAN, LANES), jnp.bfloat16),
             pltpu.VMEM((ROWS, DEPTH), jnp.bfloat16),
             pltpu.VMEM((DEPTH, DEPTH), jnp.bfloat16),
             dma((3,)),
@@ -361,7 +381,8 @@
 RING = 8
 PIECE = 8
 WIDE = 2 * LANES
-MID = DEPTH // 2
+PARTS = 4
+PART = DEPTH // PARTS
 Z_ORDER = [0, -1, 1, -2, 2, -3, 3, 4]
 Z_PLACE = {d: k for k, d in enumerate(Z_ORDER)}
 
@@ -548,63 +569,82 @@
                 high, found, preferred_element_type=jnp.float32
             ) + jnp.dot(low, found, preferred_element_type=jnp.float32)
 
-    def step(j, carry):
-        for k, at in enumerate((0, 1, 3, 5, 7)):
-            @pl.when(j == at)
-            def _():
-                ring_event(k)
-
-        zj = mod(z + pick(j, Z_ORDER), RING)
-        chunk_part(2 * zj + core, own_part, j)
-        fwd_copy(j, 0).wait_recv()
-        chunk_part(2 * zj + (1 - core), pair_out, j)
-        pair_copy(j).start()
-
-        @pl.when(j >= 1)
-        def _():
-            push_results(j - 1)
-
-        @pl.when(j >= 3)
-        def _():
-            combine(j - 3)
-
-        return carry
-
-    lax.fori_loop(0, RING, step, 0)
-    push_results(RING - 1)
-
-    def late(j, carry):
-        combine(j)
-        return carry
-
-    lax.fori_loop(RING - 3, RING, late, 0)
-
     def sum_copy(way, r, h):
-        cols = slice(h * MID, (h + 1) * MID)
+        cols = slice(h * PART, (h + 1) * PART)
         return remote(
             sum_out.at[way, r, :, cols], sum_in.at[way, r, :, cols],
             sum_send.at[way, r, h], sum_recv.at[way, r, h], at_z(-1 if way == 0 else 1),
         )
 
+    def far(way, h):
+        return (h >= PARTS // 2) == (way == 1)
+
+    def sum_steps(r, some):
+        for h in range(PARTS // 2):
+            for way in range(2):
+                sum_step(way, r, h + PARTS // 2 * int((way == 1) == some))
+
     def sum_step(way, r, h):
-        cols = slice(h * MID, (h + 1) * MID)
+        cols = slice(h * PART, (h + 1) * PART)
         d = 4 if r == 0 else (r - 4 if way == 0 else 4 - r)
         value = red[Z_PLACE[d], :, cols]
-        if r > 1 or (r == 1 and h == way):
+        if r > 1 or (r == 1 and far(way, h)):
             sum_copy(way, r - 1, h).wait_recv()
             value = value + sum_in[way, r - 1, :, cols].astype(jnp.float32)
         sum_out[way, r, :, cols] = value.astype(jnp.bfloat16)
         sum_copy(way, r, h).start()
 
-    sum_step(0, 0, 0)
-    sum_step(1, 0, 1)
-    for r in range(1, 4):
-        sum_step(0, r, 1)
-        sum_step(1, r, 0)
-        sum_step(0, r, 0)
-        sum_step(1, r, 1)
-    for h in range(2):
-        cols = slice(h * MID, (h + 1) * MID)
+    def pair_round(first, last):
+        def one(j, carry):
+            zj = mod(z + pick(j, Z_ORDER), RING)
+            chunk_part(2 * zj + core, own_part, j)
+            fwd_copy(j, 0).wait_recv()
+            chunk_part(2 * zj + (1 - core), pair_out, j)
+            pair_copy(j).start()
+
+            @pl.when(j > first)
+            def _():
+                push_results(first)
+
+            return carry
+
+        lax.fori_loop(first, last + 1, one, 0)
+        push_results(last)
+
+    def combine_some(first, last):
+        def one(j, carry):
+            combine(j)
+            return carry
+
+        lax.fori_loop(first, last + 1, one, 0)
+
+    def step(k, carry):
+        for at in range(5):
+            @pl.when(k == at)
+            def _():
+                ring_event(at)
+
+        last = jnp.minimum(2 * k, RING - 1)
+        pair_round(jnp.maximum(2 * k - 1, 0), last)
+
+        @pl.when(k >= 2)
+        def _():
+            combine_some(jnp.maximum(2 * k - 5, 0), 2 * k - 4)
+
+        return carry
+
+    lax.fori_loop(0, 5, step, 0)
+    combine_some(5, 6)
+    sum_steps(1, False)
+    combine_some(7, 7)
+    sum_steps(0, True)
+    sum_steps(2, False)
+    sum_steps(1, True)
+    sum_steps(3, False)
+    sum_steps(2, True)
+    sum_steps(3, True)
+    for h in range(PARTS):
+        cols = slice(h * PART, (h + 1) * PART)
         total = updated_ref[:, cols].astype(jnp.float32) + red[0, :, cols]
         for way in range(2):
             sum_copy(way, 3, h).wait_recv()
@@ -638,8 +678,8 @@
         for m in range(7):
             ring_copy(way, m, 0, 0).wait_send()
         for r in range(4):
-            for h in range(2):
-                if r > 0 or h == way:
+            for h in range(PARTS):
+                if r > 0 or far(way, h):
                     sum_copy(way, r, h).wait_send()
 
 
@@ -682,8 +722,8 @@
             dma((RING, N_SP)),
             dma((RING,)),
             dma((RING,)),
-            dma((2, 4, 2)),
-            dma((2, 4, 2)),
+            dma((2, 4, PARTS)),
+            dma((2, 4, PARTS)),
         ],
         compiler_params=pltpu.CompilerParams(
             collective_id=1, has_side_effects=True, vmem_limit_bytes=56 * 1024 * 1024
@@ -697,8 +737,9 @@
     expert_ids, route_weights, gate_weight, up_weight, down_weight,
 ):
     q = queries.reshape(N_SP, ROWS, LANES)
+    across = head_values.reshape(SPAN // LANES, LANES, LANES).swapaxes(1, 2)
     kv = jnp.stack(
-        [key_pairs.reshape(2, HALF, LANES), head_values.reshape(2, HALF, LANES)], axis=1
+        [key_pairs.reshape(2, HALF, LANES), across.reshape(2, HALF, LANES)], axis=1
     )
     flat_ids = expert_ids.reshape(-1)
     routes = flat_ids.shape[0]

time: 221 us -> 183 us (0.83)
  Pallas kernels: 212 us -> 174 us
    pallas_call x1, Pallas kernels: 104 us -> 74.9 us  [attend(): pl.pallas_call(attend_kernel, out_shape=(jax.ShapeDtypeStruct((ROWS, DEPT...]
    pallas_call x1, Pallas kernels: 108 us -> 98.7 us  [experts(): pl.pallas_call(expert_kernel, out_shape=jax.ShapeDtypeStruct((ROWS, DEPTH...]
where the time goes in v3:
time: 183 us; the launch traced here: 182 us
  Pallas kernels  174 us (95%)
  local copies, waits for them, and re-layouts  4.53 us (2%)
  other arithmetic  3.4 us (2%)
    pallas_call x1, Pallas kernels, experts(): pl.pallas_call(expert_kernel, out_shape=jax.ShapeDtypeStruct((ROWS, DEPTH...  98.7 us
    pallas_call x1, Pallas kernels, attend(): pl.pallas_call(attend_kernel, out_shape=(jax.ShapeDtypeStruct((ROWS, DEPT...  74.9 us

profile of v3, /device:TPU:2, one launch (start us, length us, event | category | flops | bytes accessed | tf_op | source)
XLA Modules:
  0.0 182.3 jit_solution(1662109902010772194)
XLA Ops:
  0.0 0.0 copy-start
  0.0 1.1 copy.30
  1.1 1.7 pad_maximum_fusion.kv_hbm
  3.5 0.8 copy.31
  4.3 0.1 eq.28
  4.4 0.2 convert_reduce_fusion
  4.6 0.1 reduce_sum.21
  4.7 0.1 copy.32
  4.8 0.7 multiply_add_fusion
  5.5 0.1 fusion
  5.6 0.7 copy.33
  6.3 74.9 %attend.1 = (bf16[48,2048]{1,0:T(8,128)(2,1)}, bf16[16,8,2048]{2,1,0:T(8,128)(2,1)}) custom-call(bf16[16,48,128]{2,1,0:T(8,128)(2,1)} %bitcast.14, bf16[2,2,384,128]{3,2,1,0:T(8,128)(2,1)} %pad_maximum_fusion.kv_hbm, bf16[2048,2048]{1,0:T(8,128)(2,1)} %w_hbm.1, f32[1,1]{1,0:T(1,128)} %bitcast.10.lam_ref, f32[1,128]{1,0:T(1,128)} %bitcast.17, ...), custom_call_target="tpu_custom_call" | custom-call | tf_op jit(solution)/shard_map/attend/pallas_call | solution.py:344
  81.2 0.0 copy-done
  81.2 0.1 select_reduce_fusion
  81.3 0.6 pad_maximum_fusion.1.comb_hbm
  81.9 98.7 %experts.1 = bf16[48,2048]{1,0:T(8,128)(2,1)} custom-call(bf16[16,8,2048]{2,1,0:T(8,128)(2,1)} %get-tuple-element.7.slots_hbm, bf16[2,2048,128]{2,1,0:T(8,128)(2,1)} %gate_hbm.1, bf16[2,2048,128]{2,1,0:T(8,128)(2,1)} %up_hbm.1, bf16[2,128,2048]{2,1,0:T(8,128)(2,1)} %down_hbm.1, bf16[48,256]{1,0:T(8,128)(2,1)} %pad_maximum_fusion.1.comb_hbm, ...), custom_call_target="tpu_custom_call" | custom-call | tf_op jit(solution)/shard_map/experts/pallas_call | solution.py:692
  180.7 1.6 copy.36
  (2 shorter events, 0.0 us)
Async XLA Ops:
  0.0 81.2 %copy-start = (f32[48,2]{0,1:T(2,128)S(1)}, f32[48,2]{0,1:T(2,128)}, u32[]{:S(2)}) copy-start(f32[48,2]{0,1:T(2,128)} %param.22) | copy-start | bytes 1156

commit v4 on v3

--- a/solution.py
+++ b/solution.py
@@ -1,5 +1,3 @@
-import functools
-
 import jax
 import jax.numpy as jnp
 from jax import lax
@@ -43,50 +41,17 @@
     return lax.rem(value + size, size)
 
 
-def attend_kernel(
-    q_hbm, kv_hbm, w_hbm, lam_ref, gain_ref, select_ref, residual_ref, norm_gain_ref,
+def attend_part(
+    lam_ref, gain_ref, select_ref, residual_ref, norm_gain_ref,
+    load_q, load_kv, load_w, send_comb, owner, keeps,
     updated_ref, slots_ref,
     q_own, q_land, qs, kvb, acc, top, score_a, score_b, weight_a, weight_b,
     own_heads, heads, w_vmem,
-    local_sem, q_send, q_recv, kv_send, kv_recv, head_send, head_recv,
+    q_send, q_recv, kv_send, kv_recv, head_send, head_recv,
 ):
     sp = lax.axis_index("sp")
     tp = lax.axis_index("tp")
     x, y = lax.rem(sp, SIDE), sp // SIDE
-
-    barrier = pltpu.get_barrier_semaphore()
-    load_w = pltpu.make_async_copy(w_hbm, w_vmem, local_sem.at[0])
-    load_w.start()
-    load_kv = pltpu.make_async_copy(kv_hbm, kvb.at[sp], local_sem.at[1])
-    load_kv.start()
-    load_q = pltpu.make_async_copy(q_hbm, q_own, local_sem.at[2])
-    load_q.start()
-
-    def greet_plane(d, carry):
-        pl.semaphore_signal(
-            barrier, inc=1, device_id=(lax.rem(sp + d, N_SP), tp), device_id_type=MESH
-        )
-        return carry
-
-    lax.fori_loop(1, N_SP, greet_plane, 0)
-
-    def owner(i, b):
-        return lax.rem(i + b, N_TP)
-
-    source = mod(tp - sp, N_SP)
-    keeps = owner(sp, sp) == tp
-
-    def greet_sources(h, carry):
-        @pl.when(jnp.logical_or(jnp.logical_not(keeps), h != tp))
-        def _():
-            pl.semaphore_signal(barrier, inc=1, device_id=(source, h), device_id_type=MESH)
-
-        return carry
-
-    lax.fori_loop(0, N_TP, greet_sources, 0)
-    pl.semaphore_wait(
-        barrier, N_SP - 1 + N_TP - jnp.where(keeps, jnp.int32(1), jnp.int32(0))
-    )
 
     load_q.wait()
 
@@ -131,6 +96,7 @@
         send(half, 1, (0, 0), None, -1, 0)
         send(half, 4, (0, 0), None, 0, 1)
         send(half, 8, (0, 0), None, 0, -1)
+    send_comb()
 
     for own in range(N_SP):
         @pl.when(sp == own)
@@ -316,128 +282,60 @@
         packed = jnp.dot(select_ref[...], normed, preferred_element_type=jnp.float32)
         slots_ref[:, :, cols] = packed.reshape(N_SP, 8, COLS).astype(jnp.bfloat16)
 
-    def drain_q(d, carry):
-        q_copy(d).wait_send()
-        return carry
-
-    lax.fori_loop(1, N_SP, drain_q, 0)
-
-    def drain_heads(g, carry):
-        @pl.when(jnp.logical_or(g != sp, jnp.logical_not(keeps)))
-        def _():
-            head_copy(g, tp).wait_send()
-
-        return carry
-
-    lax.fori_loop(0, N_SP, drain_heads, 0)
-    for half in range(2):
-        for index in range(20):
-            part = None if index in (0, 1) or 4 <= index < 12 else 0
-            kv_copy(half, index, sp, part, 1, 0).wait_send()
-
-
-def attend(q, kv, w, lam, gain, select, residual, norm_gain):
-    anywhere = pl.BlockSpec(memory_space=pl.ANY)
-    vmem = pl.BlockSpec(memory_space=pltpu.VMEM)
-    smem = pl.BlockSpec(memory_space=pltpu.SMEM)
-    dma = pltpu.SemaphoreType.DMA
-    return pl.pallas_call(
-        attend_kernel,
-        out_shape=(
-            jax.ShapeDtypeStruct((ROWS, DEPTH), jnp.bfloat16),
-            jax.ShapeDtypeStruct((N_SP, 8, DEPTH), jnp.bfloat16),
-        ),
-        in_specs=[anywhere, anywhere, anywhere, smem, vmem, vmem, vmem, vmem],
-        out_specs=(vmem, vmem),
-        scratch_shapes=[
-            pltpu.VMEM((N_SP, ROWS, LANES), jnp.bfloat16),
-            pltpu.VMEM((SPAN, LANES), jnp.bfloat16),
-            pltpu.VMEM((TILES, 2 * LANES, LANES), jnp.bfloat16),
-            pltpu.VMEM((N_SP, 2, 2, HALF, LANES), jnp.bfloat16),
-            pltpu.VMEM((TILES, LANES + ONES, 2 * LANES), jnp.float32),
-            pltpu.VMEM((TILES, 1, 2 * LANES), jnp.float32),
-            pltpu.VMEM((HALF, 2 * LANES), jnp.float32),
-            pltpu.VMEM((HALF, 2 * LANES), jnp.float32),
-            pltpu.VMEM((HALF, 2 * LANES), jnp.bfloat16),
-            pltpu.VMEM((HALF, 2 * LANES), jnp.bfloat16),
-            pltpu.VMEM((SPAN, LANES), jnp.bfloat16),
-            pltpu.VMEM((ROWS, DEPTH), jnp.bfloat16),
-            pltpu.VMEM((DEPTH, DEPTH), jnp.bfloat16),
-            dma((3,)),
-            dma((N_SP,)),
-            dma((N_SP,)),
-            dma((2, 20)),
-            dma((2, 20)),
-            dma((N_SP,)),
-            dma((N_TP,)),
-        ],
-        compiler_params=pltpu.CompilerParams(
-            collective_id=0, has_side_effects=True, vmem_limit_bytes=56 * 1024 * 1024
-        ),
-        name="attend",
-    )(q, kv, w, lam, gain, select, residual, norm_gain)
+    def drain():
+        def drain_q(d, carry):
+            q_copy(d).wait_send()
+            return carry
+
+        lax.fori_loop(1, N_SP, drain_q, 0)
+
+        def drain_heads(g, carry):
+            @pl.when(jnp.logical_or(g != sp, jnp.logical_not(keeps)))
+            def _():
+                head_copy(g, tp).wait_send()
+
+            return carry
+
+        lax.fori_loop(0, N_SP, drain_heads, 0)
+        for half in range(2):
+            for index in range(20):
+                part = None if index in (0, 1) or 4 <= index < 12 else 0
+                kv_copy(half, index, sp, part, 1, 0).wait_send()
+
+    return drain
 
 
 RING = 8
 PIECE = 8
 WIDE = 2 * LANES
+EARLY = 1536
+LATE = DEPTH - EARLY
 PARTS = 4
-PART = DEPTH // PARTS
+PART = EARLY // PARTS
+LATE_PART = LATE // 2
 Z_ORDER = [0, -1, 1, -2, 2, -3, 3, 4]
+SPREAD = [0, 1, 3, 4, 12, 5, 7, 8, 13, 15, 2, 6, 9, 11, 14, 10]
 Z_PLACE = {d: k for k, d in enumerate(Z_ORDER)}
 
 
-def expert_kernel(
-    slots_hbm, gate_hbm, up_hbm, down_hbm, comb_hbm, updated_ref,
+def expert_part(
+    slots_own, updated_ref, loads, comb_copy,
     merged_ref,
-    slots_own, rows, gate_up, down, comb_own, comb, own_part, pair_out, pair_in, out,
-    res, red, sum_out, sum_in,
-    local_sem, slot_send, slot_recv, ring_send, ring_recv, fwd_send, fwd_recv,
-    pair_send, pair_recv, res_send, res_recv, comb_send, comb_recv, sum_send, sum_recv,
+    rows, gate_up, down, comb, own_part, pair_out, pair_in, out,
+    res, red, sum_out, sum_in, tail_out, tail_in, whole_out, whole_in,
+    slot_send, slot_recv, ring_send, ring_recv, fwd_send, fwd_recv,
+    pair_send, pair_recv, res_send, res_recv, sum_send, sum_recv,
+    tail_send, tail_recv, whole_send, whole_recv,
 ):
     sp = lax.axis_index("sp")
     tp = lax.axis_index("tp")
     z, core = tp // 2, lax.rem(tp, 2)
-
-    barrier = pltpu.get_barrier_semaphore()
-
-    def load(k, src, dst):
-        return pltpu.make_async_copy(src, dst, local_sem.at[k])
-
-    loads = [
-        load(0, slots_hbm, slots_own),
-        load(1, slots_hbm.at[sp], rows.at[tp, sp]),
-        load(2, comb_hbm, comb_own),
-        load(3, comb_hbm, comb.at[z]),
-    ]
-    for e in range(2):
-        loads += [
-            load(4 + e, gate_hbm.at[e], gate_up.at[:, e * LANES : (e + 1) * LANES]),
-            load(6 + e, up_hbm.at[e], gate_up.at[:, (2 + e) * LANES : (3 + e) * LANES]),
-            load(8 + e, down_hbm.at[e], down.at[e * LANES : (e + 1) * LANES]),
-        ]
-    for item in loads:
-        item.start()
-
-    def greet_plane(d, carry):
-        pl.semaphore_signal(
-            barrier, inc=1, device_id=(lax.rem(sp + d, N_SP), tp), device_id_type=MESH
-        )
-        return carry
-
-    lax.fori_loop(1, N_SP, greet_plane, 0)
+    x, y = lax.rem(sp, SIDE), sp // SIDE
 
     def at_z(dz):
         return (sp, 2 * mod(z + dz, RING) + core)
 
-    def greet_ring(d, carry):
-        pl.semaphore_signal(barrier, inc=1, device_id=at_z(d), device_id_type=MESH)
-        return carry
-
-    lax.fori_loop(1, RING, greet_ring, 0)
     partner = (sp, 2 * z + (1 - core))
-    pl.semaphore_signal(barrier, inc=1, device_id=partner, device_id_type=MESH)
-    pl.semaphore_wait(barrier, N_SP - 1 + RING - 1 + 1)
 
     def remote(src, dst, send_sem, recv_sem, device):
         return pltpu.make_async_remote_copy(
@@ -445,30 +343,22 @@
             device_id=device, device_id_type=MESH,
         )
 
+    def peer(d):
+        return mod(y + d // SIDE, SIDE) * SIDE + mod(x + lax.rem(d, SIDE), SIDE)
+
     def slot_copy(d):
-        other = lax.rem(sp + d, N_SP)
+        other = peer(d)
         return remote(
             slots_own.at[other], rows.at[tp, sp], slot_send.at[d], slot_recv.at[d], (other, tp)
         )
 
-    loads[0].wait()
-
-    def send_slot(d, carry):
-        slot_copy(d).start()
+    def send_slot(n, carry):
+        slot_copy(pick(n, SPREAD)).start()
         return carry
 
     lax.fori_loop(1, N_SP, send_slot, 0)
-    loads[2].wait()
-
-    def comb_copy(d):
-        return remote(comb_own, comb.at[z], comb_send.at[d], comb_recv.at[d], at_z(d))
-
-    def send_comb(d, carry):
-        comb_copy(d).start()
-        return carry
-
-    lax.fori_loop(1, RING, send_comb, 0)
-    for item in loads[1:2] + loads[3:]:
+    rows[tp, sp] = slots_own[sp]
+    for item in loads:
         item.wait()
 
     def ring_copy(way, m, dz, piece):
@@ -485,16 +375,17 @@
         return remote(pair_out.at[j], pair_in.at[j], pair_send.at[j], pair_recv.at[j], partner)
 
     def res_copy(j, d):
-        other = lax.rem(sp + d, N_SP)
+        other = peer(d)
         return remote(
-            out.at[j, other], res.at[j, sp], res_send.at[j, d], res_recv.at[j, d], (other, tp)
+            out.at[j, other, :, 0:EARLY], res.at[j, sp, :, 0:EARLY],
+            res_send.at[j, d], res_recv.at[j, d], (other, tp),
         )
 
     def ring_event(k):
         if k == 0:
             for piece in range(2):
                 def wait_slot(src, carry):
-                    d = mod(sp - src, N_SP)
+                    d = mod(y - src // SIDE, SIDE) * SIDE + mod(x - lax.rem(src, SIDE), SIDE)
 
                     @pl.when(d != 0)
                     def _():
@@ -541,10 +432,10 @@
         pair_copy(j).wait_recv()
         total = own_part[j].astype(jnp.float32) + pair_in[j].astype(jnp.float32)
         out[j] = total.astype(jnp.bfloat16)
-        res[j, sp] = out[j, sp]
-
-        def push(d, carry):
-            res_copy(j, d).start()
+        res[j, sp, :, 0:EARLY] = out[j, sp, :, 0:EARLY]
+
+        def push(n, carry):
+            res_copy(j, pick(n, SPREAD)).start()
             return carry
 
         lax.fori_loop(1, N_SP, push, 0)
@@ -562,12 +453,57 @@
             comb_copy(mod(z - zj, RING)).wait_recv()
 
         high, low = comb[zj, :, 0:LANES], comb[zj, :, LANES:WIDE]
-        for n in range(DEPTH // COLS):
+        for n in range(EARLY // COLS):
             cols = slice(n * COLS, (n + 1) * COLS)
             found = res[j, :, :, cols].reshape(SLOTS, COLS)
             red[j, :, cols] = jnp.dot(
                 high, found, preferred_element_type=jnp.float32
             ) + jnp.dot(low, found, preferred_element_type=jnp.float32)
+
+    def tail_copy(way, r, h):
+        cols = slice(h * LATE_PART, (h + 1) * LATE_PART)
+        return remote(
+            tail_out.at[way, r, :, :, cols], tail_in.at[way, r, :, :, cols],
+            tail_send.at[way, r, h], tail_recv.at[way, r, h], at_z(-1 if way == 0 else 1),
+        )
+
+    def tail_step(way, r, h):
+        cols = slice(h * LATE_PART, (h + 1) * LATE_PART)
+        d = 4 if r == 0 else (r - 4 if way == 0 else 4 - r)
+        value = out[Z_PLACE[d], :, :, EARLY + h * LATE_PART : EARLY + (h + 1) * LATE_PART]
+        if r > 1 or (r == 1 and h == way):
+            tail_copy(way, r - 1, h).wait_recv()
+            there = tail_in[way, r - 1, :, :, cols].astype(jnp.float32)
+            value = (value.astype(jnp.float32) + there).astype(jnp.bfloat16)
+        tail_out[way, r, :, :, cols] = value
+        tail_copy(way, r, h).start()
+
+    def tail_steps(r, some):
+        for way in range(2):
+            tail_step(way, r, way if some else 1 - way)
+
+    def whole_copy(d):
+        other = peer(d)
+        return remote(
+            whole_out.at[other], whole_in.at[sp], whole_send.at[d], whole_recv.at[d], (other, tp)
+        )
+
+    def push_whole():
+        for h in range(2):
+            cols = slice(h * LATE_PART, (h + 1) * LATE_PART)
+            at = slice(EARLY + h * LATE_PART, EARLY + (h + 1) * LATE_PART)
+            total = out[0, :, :, at].astype(jnp.float32)
+            for way in range(2):
+                tail_copy(way, 3, h).wait_recv()
+                total = total + tail_in[way, 3, :, :, cols].astype(jnp.float32)
+            whole_out[:, :, cols] = total.astype(jnp.bfloat16)
+        whole_in[sp] = whole_out[sp]
+
+        def push(n, carry):
+            whole_copy(pick(n, SPREAD)).start()
+            return carry
+
+        lax.fori_loop(1, N_SP, push, 0)
 
     def sum_copy(way, r, h):
         cols = slice(h * PART, (h + 1) * PART)
@@ -627,22 +563,43 @@
         last = jnp.minimum(2 * k, RING - 1)
         pair_round(jnp.maximum(2 * k - 1, 0), last)
 
-        @pl.when(k >= 2)
+        @pl.when(jnp.logical_or(k == 2, k == 3))
         def _():
             combine_some(jnp.maximum(2 * k - 5, 0), 2 * k - 4)
 
         return carry
 
     lax.fori_loop(0, 5, step, 0)
-    combine_some(5, 6)
+    tail_steps(1, False)
+    tail_steps(0, True)
+    combine_some(3, 4)
+    tail_steps(2, False)
+    tail_steps(1, True)
+    combine_some(5, 5)
+    tail_steps(3, False)
+    tail_steps(2, True)
+    combine_some(6, 6)
+    tail_steps(3, True)
     sum_steps(1, False)
     combine_some(7, 7)
     sum_steps(0, True)
+    push_whole()
     sum_steps(2, False)
     sum_steps(1, True)
     sum_steps(3, False)
     sum_steps(2, True)
     sum_steps(3, True)
+
+    def wait_whole(d, carry):
+        whole_copy(d).wait_recv()
+        return carry
+
+    lax.fori_loop(1, N_SP, wait_whole, 0)
+    found = whole_in[...].reshape(SLOTS, LATE)
+    total = updated_ref[:, EARLY:DEPTH].astype(jnp.float32)
+    for part in (comb[z, :, 0:LANES], comb[z, :, LANES:WIDE]):
+        total = total + jnp.dot(part, found, preferred_element_type=jnp.float32)
+    merged_ref[:, EARLY:DEPTH] = total.astype(jnp.bfloat16)
     for h in range(PARTS):
         cols = slice(h * PART, (h + 1) * PART)
         total = updated_ref[:, cols].astype(jnp.float32) + red[0, :, cols]
@@ -653,6 +610,7 @@
 
     def drain_plane(d, carry):
         slot_copy(d).wait_send()
+        whole_copy(d).wait_send()
 
         def drain_res(j, inner):
             res_copy(j, d).wait_send()
@@ -661,12 +619,6 @@
         return lax.fori_loop(0, RING, drain_res, carry)
 
     lax.fori_loop(1, N_SP, drain_plane, 0)
-
-    def drain_comb(d, carry):
-        comb_copy(d).wait_send()
-        return carry
-
-    lax.fori_loop(1, RING, drain_comb, 0)
 
     def drain_pair(j, carry):
         fwd_copy(j, 0).wait_send()
@@ -678,23 +630,159 @@
         for m in range(7):
             ring_copy(way, m, 0, 0).wait_send()
         for r in range(4):
+            for h in range(2):
+                if r > 0 or h == way:
+                    tail_copy(way, r, h).wait_send()
             for h in range(PARTS):
                 if r > 0 or far(way, h):
                     sum_copy(way, r, h).wait_send()
 
 
-def experts(slots, gate, up, down, comb, updated):
+def layer_kernel(
+    q_hbm, kv_hbm, w_hbm, gate_hbm, up_hbm, down_hbm, comb_hbm,
+    lam_ref, gain_ref, select_ref, residual_ref, norm_gain_ref,
+    merged_ref,
+    *scratch,
+):
+    (q_own, q_land, qs, kvb, acc, top, score_a, score_b, weight_a, weight_b,
+     own_heads, heads, w_vmem, updated_ref, slots_own,
+     rows, gate_up, down, comb_own, comb, own_part, pair_out, pair_in, out,
+     res, red, sum_out, sum_in, tail_out, tail_in, whole_out, whole_in,
+     local_sem, q_send, q_recv, kv_send, kv_recv, head_send, head_recv,
+     slot_send, slot_recv, ring_send, ring_recv, fwd_send, fwd_recv,
+     pair_send, pair_recv, res_send, res_recv, comb_send, comb_recv, sum_send, sum_recv,
+     tail_send, tail_recv, whole_send, whole_recv) = scratch
+    sp = lax.axis_index("sp")
+    tp = lax.axis_index("tp")
+    z, core = tp // 2, lax.rem(tp, 2)
+
+    barrier = pltpu.get_barrier_semaphore()
+
+    def load(k, src, dst):
+        return pltpu.make_async_copy(src, dst, local_sem.at[k])
+
+    load_q = load(0, q_hbm, q_own)
+    load_kv = load(1, kv_hbm, kvb.at[sp])
+    load_comb = [load(2, comb_hbm, comb_own), load(3, comb_hbm, comb.at[z])]
+    load_w = load(4, w_hbm, w_vmem)
+    loads = []
+    for e in range(2):
+        loads += [
+            load(5 + e, gate_hbm.at[e], gate_up.at[:, e * LANES : (e + 1) * LANES]),
+            load(7 + e, up_hbm.at[e], gate_up.at[:, (2 + e) * LANES : (3 + e) * LANES]),
+            load(9 + e, down_hbm.at[e], down.at[e * LANES : (e + 1) * LANES]),
+        ]
+    for item in [load_q, load_kv, *load_comb, load_w, *loads]:
+        item.start()
+
+    def greet(*device):
+        pl.semaphore_signal(barrier, inc=1, device_id=device, device_id_type=MESH)
+
+    def greet_plane(d, carry):
+        greet(lax.rem(sp + d, N_SP), tp)
+        return carry
+
+    lax.fori_loop(1, N_SP, greet_plane, 0)
+
+    def owner(i, b):
+        return lax.rem(i + b, N_TP)
+
+    source = mod(tp - sp, N_SP)
+    keeps = owner(sp, sp) == tp
+
+    def greet_sources(h, carry):
+        @pl.when(jnp.logical_or(jnp.logical_not(keeps), h != tp))
+        def _():
+            greet(source, h)
+
+        return carry
+
+    lax.fori_loop(0, N_TP, greet_sources, 0)
+
+    def plane_z(d):
+        return 2 * lax.rem(z + d, RING) + core
+
+    def greet_ring(d, carry):
+        greet(sp, plane_z(d))
+        return carry
+
+    lax.fori_loop(1, RING, greet_ring, 0)
+    greet(sp, 2 * z + (1 - core))
+    pl.semaphore_wait(
+        barrier,
+        N_SP - 1 + N_TP + RING - jnp.where(keeps, jnp.int32(1), jnp.int32(0)),
+    )
+
+    def comb_copy(d):
+        return pltpu.make_async_remote_copy(
+            src_ref=comb_own, dst_ref=comb.at[z],
+            send_sem=comb_send.at[d], recv_sem=comb_recv.at[d],
+            device_id=(sp, plane_z(d)), device_id_type=MESH,
+        )
+
+    def send_comb():
+        for item in load_comb:
+            item.wait()
+
+        def one(d, carry):
+            comb_copy(d).start()
+            return carry
+
+        lax.fori_loop(1, RING, one, 0)
+
+    drain_attend = attend_part(
+        lam_ref, gain_ref, select_ref, residual_ref, norm_gain_ref,
+        load_q, load_kv, load_w, send_comb, owner, keeps,
+        updated_ref, slots_own,
+        q_own, q_land, qs, kvb, acc, top, score_a, score_b, weight_a, weight_b,
+        own_heads, heads, w_vmem,
+        q_send, q_recv, kv_send, kv_recv, head_send, head_recv,
+    )
+    expert_part(
+        slots_own, updated_ref, loads, comb_copy,
+        merged_ref,
+        rows, gate_up, down, comb, own_part, pair_out, pair_in, out,
+        res, red, sum_out, sum_in, tail_out, tail_in, whole_out, whole_in,
+        slot_send, slot_recv, ring_send, ring_recv, fwd_send, fwd_recv,
+        pair_send, pair_recv, res_send, res_recv, sum_send, sum_recv,
+        tail_send, tail_recv, whole_send, whole_recv,
+    )
+    drain_attend()
+
+    def drain_comb(d, carry):
+        comb_copy(d).wait_send()
+        return carry
+
+    lax.fori_loop(1, RING, drain_comb, 0)
+
+
+def layer(q, kv, w, gate, up, down, comb, lam, gain, select, residual, norm_gain):
     anywhere = pl.BlockSpec(memory_space=pl.ANY)
     vmem = pl.BlockSpec(memory_space=pltpu.VMEM)
+    smem = pl.BlockSpec(memory_space=pltpu.SMEM)
     dma = pltpu.SemaphoreType.DMA
     chunk = (N_SP, 8, DEPTH)
     bf16, f32 = jnp.bfloat16, jnp.float32
     return pl.pallas_call(
-        expert_kernel,
+        layer_kernel,
         out_shape=jax.ShapeDtypeStruct((ROWS, DEPTH), bf16),
-        in_specs=[anywhere] * 5 + [vmem],
+        in_specs=[anywhere] * 7 + [smem, vmem, vmem, vmem, vmem],
         out_specs=vmem,
         scratch_shapes=[
+            pltpu.VMEM((N_SP, ROWS, LANES), bf16),
+            pltpu.VMEM((SPAN, LANES), bf16),
+            pltpu.VMEM((TILES, 2 * LANES, LANES), bf16),
+            pltpu.VMEM((N_SP, 2, 2, HALF, LANES), bf16),
+            pltpu.VMEM((TILES, LANES + ONES, 2 * LANES), f32),
+            pltpu.VMEM((TILES, 1, 2 * LANES), f32),
+            pltpu.VMEM((HALF, 2 * LANES), f32),
+            pltpu.VMEM((HALF, 2 * LANES), f32),
+            pltpu.VMEM((HALF, 2 * LANES), bf16),
+            pltpu.VMEM((HALF, 2 * LANES), bf16),
+            pltpu.VMEM((SPAN, LANES), bf16),
+            pltpu.VMEM((ROWS, DEPTH), bf16),
+            pltpu.VMEM((DEPTH, DEPTH), bf16),
+            pltpu.VMEM((ROWS, DEPTH), bf16),
             pltpu.VMEM(chunk, bf16),
             pltpu.VMEM((N_TP, *chunk), bf16),
             pltpu.VMEM((DEPTH, 2 * WIDE), bf16),
@@ -706,10 +794,20 @@
             pltpu.VMEM((RING, *chunk), bf16),
             pltpu.VMEM((RING, *chunk), bf16),
             pltpu.VMEM((RING, *chunk), bf16),
-            pltpu.VMEM((RING, ROWS, DEPTH), f32),
-            pltpu.VMEM((2, 4, ROWS, DEPTH), bf16),
-            pltpu.VMEM((2, 4, ROWS, DEPTH), bf16),
-            dma((10,)),
+            pltpu.VMEM((RING, ROWS, EARLY), f32),
+            pltpu.VMEM((2, 4, ROWS, EARLY), bf16),
+            pltpu.VMEM((2, 4, ROWS, EARLY), bf16),
+            pltpu.VMEM((2, 4, N_SP, 8, LATE), bf16),
+            pltpu.VMEM((2, 4, N_SP, 8, LATE), bf16),
+            pltpu.VMEM((N_SP, 8, LATE), bf16),
+            pltpu.VMEM((N_SP, 8, LATE), bf16),
+            dma((11,)),
+            dma((N_SP,)),
+            dma((N_SP,)),
+            dma((2, 20)),
+            dma((2, 20)),
+            dma((N_SP,)),
+            dma((N_TP,)),
             dma((N_SP,)),
             dma((N_SP,)),
             dma((2, 7)),
@@ -724,12 +822,16 @@
             dma((RING,)),
             dma((2, 4, PARTS)),
             dma((2, 4, PARTS)),
+            dma((2, 4, 2)),
+            dma((2, 4, 2)),
+            dma((N_SP,)),
+            dma((N_SP,)),
         ],
         compiler_params=pltpu.CompilerParams(
-            collective_id=1, has_side_effects=True, vmem_limit_bytes=56 * 1024 * 1024
+            collective_id=0, has_side_effects=True, vmem_limit_bytes=63 * 1024 * 1024
         ),
-        name="experts",
-    )(slots, gate, up, down, comb, updated)
+        name="layer",
+    )(q, kv, w, gate, up, down, comb, lam, gain, select, residual, norm_gain)
 
 
 def shards(
@@ -752,13 +854,10 @@
     weight = jnp.sum(jnp.where(hit, route_weights[:, :, None], 0.0), axis=1)
     high = weight.astype(jnp.bfloat16)
     low = (weight - high.astype(jnp.float32)).astype(jnp.bfloat16)
-    updated, outgoing = attend(
-        q, kv, out_weight, lambdas.reshape(1, 1), head_gain.reshape(1, LANES), select,
-        residual, norm_gain.reshape(1, DEPTH),
-    )
-    return experts(
-        outgoing, gate_weight, up_weight, down_weight, jnp.concatenate([high, low], axis=1),
-        updated,
+    return layer(
+        q, kv, out_weight, gate_weight, up_weight, down_weight,
+        jnp.concatenate([high, low], axis=1), lambdas.reshape(1, 1),
+        head_gain.reshape(1, LANES), select, residual, norm_gain.reshape(1, DEPTH),
     )
 
 

time: 183 us -> 176 us (0.962)
  Pallas kernels: 174 us -> 165 us
    pallas_call x2 -> x1, Pallas kernels: 174 us -> 165 us  [layer(): pl.pallas_call(layer_kernel, out_shape=jax.ShapeDtypeStruct((ROWS, DEPTH)...]
where the time goes in v4:
time: 176 us; the launch traced here: 174 us
  Pallas kernels  165 us (94%)
  local copies, waits for them, and re-layouts  4.51 us (3%)
  other arithmetic  4.05 us (2%)
    pallas_call x1, Pallas kernels, layer(): pl.pallas_call(layer_kernel, out_shape=jax.ShapeDtypeStruct((ROWS, DEPTH)...  165 us

profile of v4, /device:TPU:2, one launch (start us, length us, event | category | flops | bytes accessed | tf_op | source)
XLA Modules:
  0.0 173.8 jit_solution(12383185698565379791)
XLA Ops:
  0.7 0.8 copy.31
  1.4 0.1 eq.28
  1.5 0.2 convert_reduce_fusion
  1.7 0.1 reduce_sum.21
  1.9 0.1 copy.32
  1.9 0.7 multiply_add_fusion
  2.6 0.1 fusion
  2.7 0.7 copy.33
  3.5 0.8 select_reduce_fusion
  4.2 0.6 pad_maximum_fusion.1.comb_hbm
  4.8 1.1 copy.30
  5.9 1.7 pad_maximum_fusion.kv_hbm
  7.6 164.5 %layer.1 = bf16[48,2048]{1,0:T(8,128)(2,1)} custom-call(bf16[16,48,128]{2,1,0:T(8,128)(2,1)} %bitcast.14, bf16[2,2,384,128]{3,2,1,0:T(8,128)(2,1)} %pad_maximum_fusion.kv_hbm, bf16[2048,2048]{1,0:T(8,128)(2,1)} %w_hbm.1, bf16[2,2048,128]{2,1,0:T(8,128)(2,1)} %gate_hbm.1, bf16[2,2048,128]{2,1,0:T(8,128)(2,1)} %up_hbm.1, bf16[2,128,2048]{2,1,0:T(8,128)(2,1)} %down_hbm.1, ...), custom_call_target="tpu_custom_call" | custom-call | tf_op jit(solution)/shard_map/layer/pallas_call | solution.py:766
  172.2 1.6 copy.36
  (2 shorter events, 0.0 us)

commit v5 on v4

--- a/solution.py
+++ b/solution.py
@@ -279,7 +279,9 @@
     for n in range(DEPTH // COLS):
         cols = slice(n * COLS, (n + 1) * COLS)
         normed = (wide[n] * scale * norm_gain_ref[:, cols]).astype(jnp.bfloat16)
-        packed = jnp.dot(select_ref[...], normed, preferred_element_type=jnp.float32)
+        packed = lax.dot_general(
+            select_ref[...], normed, (((0,), (0,)), ((), ())), preferred_element_type=jnp.float32
+        )
         slots_ref[:, :, cols] = packed.reshape(N_SP, 8, COLS).astype(jnp.bfloat16)
 
     def drain():
@@ -843,15 +845,15 @@
     kv = jnp.stack(
         [key_pairs.reshape(2, HALF, LANES), across.reshape(2, HALF, LANES)], axis=1
     )
-    flat_ids = expert_ids.reshape(-1)
-    routes = flat_ids.shape[0]
-    same = flat_ids[:, None] == flat_ids[None, :]
-    earlier = jnp.arange(routes)[:, None] > jnp.arange(routes)[None, :]
-    ranking = jnp.sum((same & earlier).astype(jnp.int32), axis=1)
-    slots = (flat_ids * CAP + ranking).reshape(ROWS, 2)
-    hit = slots[:, :, None] == jnp.arange(SLOTS, dtype=jnp.int32)[None, None, :]
-    select = jnp.any(hit, axis=1).T.astype(jnp.bfloat16)
-    weight = jnp.sum(jnp.where(hit, route_weights[:, :, None], 0.0), axis=1)
+    slot = jnp.arange(SLOTS, dtype=jnp.int32)[None, :]
+    first, second = (expert_ids[:, c : c + 1] == slot // CAP for c in range(2))
+    named = first | second
+    earlier = jnp.tri(ROWS, k=-1, dtype=jnp.bfloat16)
+    rank = jnp.dot(earlier, named.astype(jnp.bfloat16), preferred_element_type=jnp.float32)
+    hit = named & (rank == (slot % CAP).astype(jnp.float32))
+    select = hit.astype(jnp.bfloat16)
+    weight = jnp.where(first, route_weights[:, 0:1], route_weights[:, 1:2])
+    weight = jnp.where(hit, weight, 0.0)
     high = weight.astype(jnp.bfloat16)
     low = (weight - high.astype(jnp.float32)).astype(jnp.bfloat16)
     return layer(

time: 176 us -> 175 us (level)
  no operation moved by 1% of the time
where the time goes in v5:
time: 175 us; the launch traced here: 173 us
  Pallas kernels  164 us (94%)
  local copies, waits for them, and re-layouts  4.22 us (2%)
  other arithmetic  3.03 us (2%)
    pallas_call x1, Pallas kernels, layer(): pl.pallas_call(layer_kernel, out_shape=jax.ShapeDtypeStruct((ROWS, DEPTH)...  164 us

profile of v5, /device:TPU:2, one launch (start us, length us, event | category | flops | bytes accessed | tf_op | source)
XLA Modules:
  0.0 172.6 jit_solution(9034578613067224933)
XLA Ops:
  0.7 0.8 slice_bitcast_fusion.3
  1.4 0.8 slice_bitcast_fusion.1
  2.2 0.2 fusion.4
  2.4 0.1 fusion.3
  2.5 0.6 pad_maximum_fusion.1.comb_hbm
  3.1 0.6 convert_element_type.26.select_ref
  3.7 1.1 copy.14
  4.8 1.7 pad_maximum_fusion.kv_hbm
  6.5 164.4 %layer.1 = bf16[48,2048]{1,0:T(8,128)(2,1)} custom-call(bf16[16,48,128]{2,1,0:T(8,128)(2,1)} %bitcast.21, bf16[2,2,384,128]{3,2,1,0:T(8,128)(2,1)} %pad_maximum_fusion.kv_hbm, bf16[2048,2048]{1,0:T(8,128)(2,1)} %w_hbm.1, bf16[2,2048,128]{2,1,0:T(8,128)(2,1)} %gate_hbm.1, bf16[2,2048,128]{2,1,0:T(8,128)(2,1)} %up_hbm.1, bf16[2,128,2048]{2,1,0:T(8,128)(2,1)} %down_hbm.1, ...), custom_call_target="tpu_custom_call" | custom-call | tf_op jit(solution)/shard_map/layer/pallas_call | solution.py:768
  171.0 1.6 copy.17
  (2 shorter events, 0.0 us)
